TPU v7x, 256 devices: a whole 4x4x8 slice. The times are simulated.
256 devices in a mesh: sp: 64 (over z, x, core), tp: 4 (over y).
Axes of the slice: x: 4, y: 4, z: 8, core: 2. Of those that a mesh axis runs over, the one named last changes fastest.
Arguments:
- queries: bfloat16 [16384, 1024], P('sp', 'tp'), may hold values from -9 to 9
- keys: bfloat16 [16384, 512], P('sp', 'tp'), may hold values from -9 to 9
- values: bfloat16 [16384, 512], P('sp', 'tp'), may hold values from -6 to 6
- residual: bfloat16 [16384, 2048], P(('sp', 'tp')), may hold values from -6 to 6
- query_gain: float32 [128], replicated, may hold values from 1 to 5
- key_gain: float32 [128], replicated, may hold values from 1 to 5
- out_weight: bfloat16 [1024, 2048], replicated, may hold values from -0.1875 to 0.1875
- first_gain: float32 [2048], replicated, may hold values from 0.1 to 1.9
- first_bias: float32 [2048], replicated, may hold values from -3 to 3
- up_weight: bfloat16 [2048, 8192], P('sp', 'tp'), may hold values from -0.125 to 0.125
- down_weight: bfloat16 [2048, 8192], P('sp', 'tp'), may hold values from -0.0625 to 0.0625
- second_gain: float32 [2048], replicated, may hold values from 0.1 to 1.9
- second_bias: float32 [2048], replicated, may hold values from -3 to 3
Outputs:
- layer_out: bfloat16 [16384, 2048], P(('sp', 'tp'))
All inputs are finite; a program needn't handle non-finite values.
Results may differ from a plain program's by a relative error of at most 0.015.
Values may be sent and summed in bfloat16 or wider, within the bound.
A program may use at most 128 MiB of HBM per device.

v0:
```python
import jax
import jax.numpy as jnp
from jax import lax
from jax.sharding import PartitionSpec as P

HEAD_DIM = 128
GRID_W = 64


RESIDUAL_SCALE = 2.0**0.25
LAYER_EPS = 1e-05
HEAD_EPS = 1e-06
ROTARY_BASE = 10000.0


def side_by_side(arrays, axis, dim, along):
    both = jnp.concatenate(arrays, axis=along)
    result, at, finished = (lax.all_gather(both, axis, axis=dim, tiled=True), 0, [])
    for a in arrays:
        finished.append(lax.slice_in_dim(result, at, at + a.shape[along], axis=along))
        at += a.shape[along]
    return tuple(finished)


def sent_to_all(x, axis):
    copies = jnp.broadcast_to(x, (lax.axis_size(axis), *x.shape))
    return lax.all_to_all(copies, axis, split_axis=0, concat_axis=0, tiled=True)


def in_order(parts, dim):
    dims = list(parts.shape[1:])
    dims[dim] *= parts.shape[0]
    return jnp.moveaxis(parts, 0, dim).reshape(dims)


def collect(x, axis, dim):
    parts = sent_to_all(x, axis)
    return in_order(parts, dim)


def split_up(x, dim, count):
    dims = x.shape
    parts = x.reshape(*dims[:dim], count, dims[dim] // count, *dims[dim + 1 :])
    return jnp.moveaxis(parts, dim, 0)


def sum_at_owner(x, axis, dim):
    parts = split_up(x, dim, lax.axis_size(axis))
    arrived = lax.all_to_all(parts, axis, split_axis=0, concat_axis=0, tiled=True)
    return arrived.astype(jnp.float32).sum(axis=0)


def grid_angles(positions, head_dim):
    quarter = head_dim // 4
    inverse = ROTARY_BASE ** (-jnp.arange(quarter, dtype=jnp.float32) / quarter)
    grid_row = (positions // GRID_W).astype(jnp.float32)
    grid_col = (positions % GRID_W).astype(jnp.float32)
    return jnp.concatenate([grid_row[:, None] * inverse, grid_col[:, None] * inverse], axis=-1)


def norm_rotate(projected, gain, angles, head_dim):
    row_count = projected.shape[0]
    head_count = projected.shape[1] // head_dim
    as_float = projected.astype(jnp.float32).reshape(row_count, head_count, head_dim)
    normed = (
        as_float
        * lax.rsqrt(jnp.mean(as_float * as_float, axis=-1, keepdims=True) + HEAD_EPS)
        * gain
    )
    paired = normed.reshape(row_count, head_count, head_dim // 2, 2)
    cosine = jnp.cos(angles)[:, None, :]
    sine = jnp.sin(angles)[:, None, :]
    even_part = paired[..., 0]
    odd_part = paired[..., 1]
    turned = jnp.stack(
        [even_part * cosine - odd_part * sine, even_part * sine + odd_part * cosine], axis=-1
    )
    return turned.reshape(row_count, head_count, head_dim).astype(jnp.bfloat16)


def layer_norm(summed, gain, bias):
    centred = summed - jnp.mean(summed, axis=-1, keepdims=True)
    variance = jnp.mean(centred * centred, axis=-1, keepdims=True)
    return centred * lax.rsqrt(variance + LAYER_EPS) * gain + bias


def attend_piece(carried, pieces, query_grp):
    key_rows, value_rows = pieces
    kv_here = query_grp.shape[1]
    head_dim = query_grp.shape[3]
    piece_rows = key_rows.shape[0]
    block_rows = 2048
    key_blocks = key_rows.reshape(piece_rows // block_rows, block_rows, kv_here, head_dim)
    value_blocks = value_rows.reshape(piece_rows // block_rows, block_rows, kv_here, head_dim)
    score_scale = head_dim ** (-0.5)

    def advance(state, blocks):
        running, total, summed = state
        key_block, value_block = blocks
        scores = (
            jnp.einsum("qkgd,skd->kgqs", query_grp, key_block, preferred_element_type=jnp.float32)
            * score_scale
        )
        newest = jnp.maximum(running, jnp.max(scores, axis=-1))
        factor = jnp.exp(running - newest)
        weights = jnp.exp(scores - newest[..., None])
        total = total * factor + jnp.sum(weights, axis=-1)
        summed = summed * factor[..., None] + jnp.einsum(
            "kgqs,skd->kgqd",
            weights.astype(jnp.bfloat16),
            value_block,
            preferred_element_type=jnp.float32,
        )
        return ((newest, total, summed), None)

    result, unused = lax.scan(advance, carried, (key_blocks, value_blocks))
    return result


def per_device(
    queries,
    keys,
    values,
    residual,
    query_gain,
    key_gain,
    out_weight,
    first_gain,
    first_bias,
    up_weight,
    down_weight,
    second_gain,
    second_bias,
):
    head_dim = HEAD_DIM
    row_count = queries.shape[0]
    positions = lax.axis_index("sp") * row_count + jnp.arange(row_count, dtype=jnp.int32)
    angles = grid_angles(positions, head_dim)
    query_rot = norm_rotate(queries, query_gain, angles, head_dim)
    key_rot = norm_rotate(keys, key_gain, angles, head_dim)
    kv_here = key_rot.shape[1]
    group = query_rot.shape[1] // kv_here
    query_grp = query_rot.reshape(row_count, kv_here, group, head_dim)
    initial = (
        jnp.full((kv_here, group, row_count), -1e30, jnp.float32),
        jnp.zeros((kv_here, group, row_count), jnp.float32),
        jnp.zeros((kv_here, group, row_count, head_dim), jnp.float32),
    )
    running, total, summed = attend_piece(
        initial,
        side_by_side((key_rot.reshape(row_count, kv_here * head_dim), values), "sp", 0, 1),
        query_grp,
    )
    attended = (
        jnp.transpose(summed / total[..., None], (2, 0, 1, 3))
        .reshape(row_count, -1)
        .astype(jnp.bfloat16)
    )
    regrouped = lax.all_to_all(attended, "tp", split_axis=0, concat_axis=1, tiled=True)
    mixed = jnp.dot(regrouped, out_weight, preferred_element_type=jnp.float32)
    whole_up, whole_down = side_by_side((up_weight, down_weight), "sp", 0, 1)
    first_norm = layer_norm(
        RESIDUAL_SCALE * residual.astype(jnp.float32) + mixed, first_gain, first_bias
    ).astype(jnp.bfloat16)
    all_rows = collect(first_norm, "tp", 0)
    up_values = jnp.dot(all_rows, whole_up, preferred_element_type=jnp.float32)
    hidden = jnp.square(jnp.maximum(up_values, 0.0)).astype(jnp.bfloat16)
    channel_out = sum_at_owner(
        lax.dot_general(
            hidden, whole_down, (((1,), (1,)), ((), ())), preferred_element_type=jnp.float32
        ).astype(jnp.bfloat16),
        "tp",
        0,
    )
    layer_out = layer_norm(
        RESIDUAL_SCALE * first_norm.astype(jnp.float32) + channel_out, second_gain, second_bias
    )
    return layer_out.astype(jnp.bfloat16)


def solution(mesh):
    in_specs = (
        P("sp", "tp"),
        P("sp", "tp"),
        P("sp", "tp"),
        P(("sp", "tp"), None),
        P(),
        P(),
        P(),
        P(),
        P(),
        P("sp", "tp"),
        P("sp", "tp"),
        P(),
        P(),
    )
    out_specs = P(("sp", "tp"), None)
    return jax.shard_map(
        per_device, mesh=mesh, in_specs=in_specs, out_specs=out_specs, check_vma=False
    )
```

profile of v0, /device:TPU:1, one launch (start us, length us, event | category | flops | bytes accessed | tf_op | source)
XLA Modules:
  0.0 247.9 jit_solution(13141953183458167844)
XLA Ops:
  6.6 1.0 fusion.44
  7.5 0.9 fusion.45
  9.3 0.9 copy.45
  10.2 0.7 pad_maximum_fusion.1
  10.9 1.7 pad_maximum_fusion
  12.7 1.0 copy.46
  13.7 0.9 convert_multiply_fusion.2
  14.8 0.3 reduce_sum.75
  15.9 0.3 subtract_convert_fusion
  16.9 83.3 %all-gather.3.cloned.1.call-done = bf16[16384,256]{0,1:T(8,128)(2,1)} async-done(((bf16[256,256]{0,1:T(8,128)(2,1)}), bf16[16384,256]{0,1:T(8,128)(2,1)}) %all-gather.3.cloned.1.call-update) | async-done | bytes 8388624 | tf_op jit(solution)/shard_map/all_gather | solution.py:18
  100.2 5.8 %fusion.57 = (bf16[16384,128]{0,1:T(8,128)(2,1)}, bf16[16384,128]{0,1:T(8,128)(2,1)}) fusion(bf16[16384,256]{0,1:T(8,128)(2,1)} %all-gather.3.cloned.1.call-done), kind=kLoop, calls=%fused_computation.88 | loop fusion | bytes 16777216 | tf_op jit(solution)/shard_map/slice | solution.py:20
  106.0 6.4 %copy.55 = bf16[16384,128]{1,0:T(8,128)(2,1)} copy(bf16[16384,128]{0,1:T(8,128)(2,1)} %get-tuple-element.109) | data formatting | bytes 8388608
  112.4 6.4 %copy.56 = bf16[16384,128]{1,0:T(8,128)(2,1)} copy(bf16[16384,128]{0,1:T(8,128)(2,1)} %get-tuple-element.108) | data formatting | bytes 8388608
  118.8 66.3 %while.15 = (s32[]{:T(128)}, f32[1,2,256]{2,1,0:T(2,128)S(1)}, f32[1,2,256]{2,1,0:T(2,128)S(1)}, f32[1,2,256,128]{3,2,1,0:T(8,128)S(1)}, bf16[8,2048,1,128]{3,1,...) while((s32[]{:T(128)}, f32[1,2,256]{2,1,0:T(2,128)S(1)}, ...), condition=%wide.region_5.6_spmd.clone, body=%wide.region_2.5_spmd.clone.sunk | while | flops 545459200 | bytes 31097988 | solution.py:116
  118.8 3.8 %bitcast_reduce_fusion.2 = (f32[2,256]{1,0:T(2,128)S(1)}, f32[2048,256,2]{1,0,2:T(8,128)}) fusion(bf16[256,1,2,128]{3,0,2,1:T(8,128)(2,1)S(1)} %get-tuple-element.202, bf16[8,2048,1,128]{3,1,2,0:T(8,128)(2,1)} %get-tuple-element.201, s32[]{:T(128)} %get-tuple-element.188), kind=kOutput, calls=%fused_computation.1.clone.1 | convolution fusion | flops 270532096 | bytes 4852224 | tf_op jit(solution)/shard_map/while/body/eval_jaxpr/qkgd,skd->kgqs/dot_general | solution.py:101
  122.6 3.3 %fusion.72 = f32[1,2,256,128]{3,2,1,0:T(8,128)S(1)} fusion(f32[2048,256,2]{1,0,2:T(8,128)} %get-tuple-element.177, f32[2,256]{1,0:T(2,128)S(1)} %bitcast.104, bf16[8,2048,1,128]{3,1,2,0:T(8,128)(2,1)} %get-tuple-element.203, s32[]{:T(128)} %get-tuple-element.188, f32[1,2,256,128]{3,2,1,0:T(8,128)S(1)} %get-tuple-element.191, ...), kind=kOutput, calls=%fused_computation.10.clone.1 | convolution fusion | flops 271777792 | bytes 5247489 | tf_op jit(solution)/shard_map/while/body/eval_jaxpr/kgqs,skd->kgqd/dot_general | solution.py:108
  126.2 0.7 fusion.71
  126.9 3.7 %bitcast_reduce_fusion.2 = (f32[2,256]{1,0:T(2,128)S(1)}, f32[2048,256,2]{1,0,2:T(8,128)}) fusion(bf16[256,1,2,128]{3,0,2,1:T(8,128)(2,1)S(1)} %get-tuple-element.202, bf16[8,2048,1,128]{3,1,2,0:T(8,128)(2,1)} %get-tuple-element.201, s32[]{:T(128)} %get-tuple-element.188), kind=kOutput, calls=%fused_computation.1.clone.1 | convolution fusion | flops 270532096 | bytes 4852224 | tf_op jit(solution)/shard_map/while/body/eval_jaxpr/qkgd,skd->kgqs/dot_general | solution.py:101
  130.7 3.4 %fusion.72 = f32[1,2,256,128]{3,2,1,0:T(8,128)S(1)} fusion(f32[2048,256,2]{1,0,2:T(8,128)} %get-tuple-element.177, f32[2,256]{1,0:T(2,128)S(1)} %bitcast.104, bf16[8,2048,1,128]{3,1,2,0:T(8,128)(2,1)} %get-tuple-element.203, s32[]{:T(128)} %get-tuple-element.188, f32[1,2,256,128]{3,2,1,0:T(8,128)S(1)} %get-tuple-element.191, ...), kind=kOutput, calls=%fused_computation.10.clone.1 | convolution fusion | flops 271777792 | bytes 5247489 | tf_op jit(solution)/shard_map/while/body/eval_jaxpr/kgqs,skd->kgqd/dot_general | solution.py:108
  134.3 0.7 fusion.71
  135.1 3.7 %bitcast_reduce_fusion.2 = (f32[2,256]{1,0:T(2,128)S(1)}, f32[2048,256,2]{1,0,2:T(8,128)}) fusion(bf16[256,1,2,128]{3,0,2,1:T(8,128)(2,1)S(1)} %get-tuple-element.202, bf16[8,2048,1,128]{3,1,2,0:T(8,128)(2,1)} %get-tuple-element.201, s32[]{:T(128)} %get-tuple-element.188), kind=kOutput, calls=%fused_computation.1.clone.1 | convolution fusion | flops 270532096 | bytes 4852224 | tf_op jit(solution)/shard_map/while/body/eval_jaxpr/qkgd,skd->kgqs/dot_general | solution.py:101
  138.8 3.3 %fusion.72 = f32[1,2,256,128]{3,2,1,0:T(8,128)S(1)} fusion(f32[2048,256,2]{1,0,2:T(8,128)} %get-tuple-element.177, f32[2,256]{1,0:T(2,128)S(1)} %bitcast.104, bf16[8,2048,1,128]{3,1,2,0:T(8,128)(2,1)} %get-tuple-element.203, s32[]{:T(128)} %get-tuple-element.188, f32[1,2,256,128]{3,2,1,0:T(8,128)S(1)} %get-tuple-element.191, ...), kind=kOutput, calls=%fused_computation.10.clone.1 | convolution fusion | flops 271777792 | bytes 5247489 | tf_op jit(solution)/shard_map/while/body/eval_jaxpr/kgqs,skd->kgqd/dot_general | solution.py:108
  142.4 0.7 fusion.71
  143.1 3.7 %bitcast_reduce_fusion.2 = (f32[2,256]{1,0:T(2,128)S(1)}, f32[2048,256,2]{1,0,2:T(8,128)}) fusion(bf16[256,1,2,128]{3,0,2,1:T(8,128)(2,1)S(1)} %get-tuple-element.202, bf16[8,2048,1,128]{3,1,2,0:T(8,128)(2,1)} %get-tuple-element.201, s32[]{:T(128)} %get-tuple-element.188), kind=kOutput, calls=%fused_computation.1.clone.1 | convolution fusion | flops 270532096 | bytes 4852224 | tf_op jit(solution)/shard_map/while/body/eval_jaxpr/qkgd,skd->kgqs/dot_general | solution.py:101
  146.9 3.3 %fusion.72 = f32[1,2,256,128]{3,2,1,0:T(8,128)S(1)} fusion(f32[2048,256,2]{1,0,2:T(8,128)} %get-tuple-element.177, f32[2,256]{1,0:T(2,128)S(1)} %bitcast.104, bf16[8,2048,1,128]{3,1,2,0:T(8,128)(2,1)} %get-tuple-element.203, s32[]{:T(128)} %get-tuple-element.188, f32[1,2,256,128]{3,2,1,0:T(8,128)S(1)} %get-tuple-element.191, ...), kind=kOutput, calls=%fused_computation.10.clone.1 | convolution fusion | flops 271777792 | bytes 5247489 | tf_op jit(solution)/shard_map/while/body/eval_jaxpr/kgqs,skd->kgqd/dot_general | solution.py:108
  150.5 0.7 fusion.71
  151.2 4.2 %bitcast_reduce_fusion.2 = (f32[2,256]{1,0:T(2,128)S(1)}, f32[2048,256,2]{1,0,2:T(8,128)}) fusion(bf16[256,1,2,128]{3,0,2,1:T(8,128)(2,1)S(1)} %get-tuple-element.202, bf16[8,2048,1,128]{3,1,2,0:T(8,128)(2,1)} %get-tuple-element.201, s32[]{:T(128)} %get-tuple-element.188), kind=kOutput, calls=%fused_computation.1.clone.1 | convolution fusion | flops 270532096 | bytes 4852224 | tf_op jit(solution)/shard_map/while/body/eval_jaxpr/qkgd,skd->kgqs/dot_general | solution.py:101
  155.4 3.3 %fusion.72 = f32[1,2,256,128]{3,2,1,0:T(8,128)S(1)} fusion(f32[2048,256,2]{1,0,2:T(8,128)} %get-tuple-element.177, f32[2,256]{1,0:T(2,128)S(1)} %bitcast.104, bf16[8,2048,1,128]{3,1,2,0:T(8,128)(2,1)} %get-tuple-element.203, s32[]{:T(128)} %get-tuple-element.188, f32[1,2,256,128]{3,2,1,0:T(8,128)S(1)} %get-tuple-element.191, ...), kind=kOutput, calls=%fused_computation.10.clone.1 | convolution fusion | flops 271777792 | bytes 5247489 | tf_op jit(solution)/shard_map/while/body/eval_jaxpr/kgqs,skd->kgqd/dot_general | solution.py:108
  159.0 0.7 fusion.71
  159.7 3.7 %bitcast_reduce_fusion.2 = (f32[2,256]{1,0:T(2,128)S(1)}, f32[2048,256,2]{1,0,2:T(8,128)}) fusion(bf16[256,1,2,128]{3,0,2,1:T(8,128)(2,1)S(1)} %get-tuple-element.202, bf16[8,2048,1,128]{3,1,2,0:T(8,128)(2,1)} %get-tuple-element.201, s32[]{:T(128)} %get-tuple-element.188), kind=kOutput, calls=%fused_computation.1.clone.1 | convolution fusion | flops 270532096 | bytes 4852224 | tf_op jit(solution)/shard_map/while/body/eval_jaxpr/qkgd,skd->kgqs/dot_general | solution.py:101
  163.5 3.3 %fusion.72 = f32[1,2,256,128]{3,2,1,0:T(8,128)S(1)} fusion(f32[2048,256,2]{1,0,2:T(8,128)} %get-tuple-element.177, f32[2,256]{1,0:T(2,128)S(1)} %bitcast.104, bf16[8,2048,1,128]{3,1,2,0:T(8,128)(2,1)} %get-tuple-element.203, s32[]{:T(128)} %get-tuple-element.188, f32[1,2,256,128]{3,2,1,0:T(8,128)S(1)} %get-tuple-element.191, ...), kind=kOutput, calls=%fused_computation.10.clone.1 | convolution fusion | flops 271777792 | bytes 5247489 | tf_op jit(solution)/shard_map/while/body/eval_jaxpr/kgqs,skd->kgqd/dot_general | solution.py:108
  166.8 0.5 copy-done
  167.3 0.7 fusion.71
  168.1 3.9 %bitcast_reduce_fusion.2 = (f32[2,256]{1,0:T(2,128)S(1)}, f32[2048,256,2]{1,0,2:T(8,128)}) fusion(bf16[256,1,2,128]{3,0,2,1:T(8,128)(2,1)S(1)} %get-tuple-element.202, bf16[8,2048,1,128]{3,1,2,0:T(8,128)(2,1)} %get-tuple-element.201, s32[]{:T(128)} %get-tuple-element.188), kind=kOutput, calls=%fused_computation.1.clone.1 | convolution fusion | flops 270532096 | bytes 4852224 | tf_op jit(solution)/shard_map/while/body/eval_jaxpr/qkgd,skd->kgqs/dot_general | solution.py:101
  172.0 3.5 %fusion.72 = f32[1,2,256,128]{3,2,1,0:T(8,128)S(1)} fusion(f32[2048,256,2]{1,0,2:T(8,128)} %get-tuple-element.177, f32[2,256]{1,0:T(2,128)S(1)} %bitcast.104, bf16[8,2048,1,128]{3,1,2,0:T(8,128)(2,1)} %get-tuple-element.203, s32[]{:T(128)} %get-tuple-element.188, f32[1,2,256,128]{3,2,1,0:T(8,128)S(1)} %get-tuple-element.191, ...), kind=kOutput, calls=%fused_computation.10.clone.1 | convolution fusion | flops 271777792 | bytes 5247489 | tf_op jit(solution)/shard_map/while/body/eval_jaxpr/kgqs,skd->kgqd/dot_general | solution.py:108
  175.5 0.6 copy-done
  176.1 0.7 fusion.71
  176.8 3.7 %bitcast_reduce_fusion.2 = (f32[2,256]{1,0:T(2,128)S(1)}, f32[2048,256,2]{1,0,2:T(8,128)}) fusion(bf16[256,1,2,128]{3,0,2,1:T(8,128)(2,1)S(1)} %get-tuple-element.202, bf16[8,2048,1,128]{3,1,2,0:T(8,128)(2,1)} %get-tuple-element.201, s32[]{:T(128)} %get-tuple-element.188), kind=kOutput, calls=%fused_computation.1.clone.1 | convolution fusion | flops 270532096 | bytes 4852224 | tf_op jit(solution)/shard_map/while/body/eval_jaxpr/qkgd,skd->kgqs/dot_general | solution.py:101
  180.6 3.4 %fusion.72 = f32[1,2,256,128]{3,2,1,0:T(8,128)S(1)} fusion(f32[2048,256,2]{1,0,2:T(8,128)} %get-tuple-element.177, f32[2,256]{1,0:T(2,128)S(1)} %bitcast.104, bf16[8,2048,1,128]{3,1,2,0:T(8,128)(2,1)} %get-tuple-element.203, s32[]{:T(128)} %get-tuple-element.188, f32[1,2,256,128]{3,2,1,0:T(8,128)S(1)} %get-tuple-element.191, ...), kind=kOutput, calls=%fused_computation.10.clone.1 | convolution fusion | flops 271777792 | bytes 5247489 | tf_op jit(solution)/shard_map/while/body/eval_jaxpr/kgqs,skd->kgqd/dot_general | solution.py:108
  184.0 0.3 copy-done
  184.3 0.7 fusion.71
  185.5 8.7 %all_to_all.26 = bf16[4,64,256]{2,1,0:T(8,128)(2,1)S(1)} all-to-all(bf16[4,64,256]{2,1,0:T(8,128)(2,1)S(1)} %convert_element_type.81), channel_id=1, replica_groups=mesh['sp'=64,'tp'=4] {'tp'}, dimensions={0} | all-to-all | bytes 262144 | tf_op jit(solution)/shard_map/all_to_all | solution.py:159
  194.2 3.2 %fusion.59 = (f32[64]{0:T(128)S(1)}, f32[64,2048]{1,0:T(8,128)S(1)}) fusion(bf16[64,1024]{1,0:T(8,128)(2,1)S(1)} %bitcast.110, bf16[1024,2048]{1,0:T(8,128)(2,1)} %param.21, bf16[64,2048]{1,0:T(8,128)(2,1)S(1)} %copy-done.1), kind=kOutput, calls=%fused_computation.90 | convolution fusion | flops 268959680 | bytes 5112064 | tf_op jit(solution)/shard_map/dot_general | solution.py:160
  198.0 15.9 %all_to_all.27 = bf16[4,64,2048]{2,1,0:T(8,128)(2,1)S(1)} all-to-all(bf16[4,64,2048]{2,1,0:T(8,128)(2,1)S(1)} %broadcast_in_dim.11), channel_id=1, replica_groups=mesh['sp'=64,'tp'=4] {'tp'}, dimensions={0} | all-to-all | bytes 2097152 | tf_op jit(solution)/shard_map/all_to_all | solution.py:27
  213.9 10.3 %fusion.37 = bf16[256,2048]{1,0:T(8,128)(2,1)S(1)} fusion(bf16[2048,4096]{1,0:T(8,128)(2,1)} %all-gather.5.cloned.1.call-done, bf16[256,2048]{1,0:T(8,128)(2,1)S(1)} %bitcast.106), kind=kOutput, calls=%fused_computation.34 | convolution fusion | flops 4297064448 | bytes 18874368 | tf_op jit(solution)/shard_map/dot_general | solution.py:169
  224.2 15.1 %all_to_all.28 = bf16[4,64,2048]{2,1,0:T(8,128)(2,1)S(1)} all-to-all(bf16[4,64,2048]{2,1,0:T(8,128)(2,1)S(1)} %bitcast.107), channel_id=1, replica_groups=mesh['sp'=64,'tp'=4] {'tp'}, dimensions={0} | all-to-all | bytes 2097152 | tf_op jit(solution)/shard_map/all_to_all | solution.py:49
  239.7 0.3 multiply_reduce_fusion
  240.1 1.0 add_convert_fusion
  (91 shorter events, 5.2 us)
Async XLA Ops:
  6.5 8.8 %copy-start.6 = (f32[128]{0:T(128)S(1)}, f32[128]{0:T(128)}, u32[]{:S(2)}) copy-start(f32[128]{0:T(128)} %param.19) | copy-start | bytes 1540
  6.5 93.7 %all-gather.3.cloned.1.call-start = ((), (), s32[]{:S(2)}) async-start(), calls=%async_computation.3 | async-start | bytes 8519680 | tf_op jit(solution)/shard_map/all_gather | solution.py:18
  10.9 203.0 %all-gather.5.cloned.1.call-start = ((), (), s32[]{:S(2)}) async-start(), calls=%async_computation.4 | async-start | bytes 17039360 | tf_op jit(solution)/shard_map/all_gather | solution.py:18
  118.8 75.5 %copy-start.1 = (bf16[64,2048]{1,0:T(8,128)(2,1)S(1)}, bf16[64,2048]{1,0:T(8,128)(2,1)}, u32[]{:S(2)}) copy-start(bf16[64,2048]{1,0:T(8,128)(2,1)} %param.18) | copy-start | bytes 786436
  122.5 3.6 %copy-start = (f32[2048,256,2]{1,0,2:T(8,128)S(1)}, f32[2048,256,2]{1,0,2:T(8,128)}, u32[]{:S(2)}) copy-start(f32[2048,256,2]{1,0,2:T(8,128)} %get-tuple-element.177) | copy-start | bytes 12582916 | tf_op jit(solution)/shard_map/while
  130.7 3.7 %copy-start = (f32[2048,256,2]{1,0,2:T(8,128)S(1)}, f32[2048,256,2]{1,0,2:T(8,128)}, u32[]{:S(2)}) copy-start(f32[2048,256,2]{1,0,2:T(8,128)} %get-tuple-element.177) | copy-start | bytes 12582916 | tf_op jit(solution)/shard_map/while
  138.8 3.6 %copy-start = (f32[2048,256,2]{1,0,2:T(8,128)S(1)}, f32[2048,256,2]{1,0,2:T(8,128)}, u32[]{:S(2)}) copy-start(f32[2048,256,2]{1,0,2:T(8,128)} %get-tuple-element.177) | copy-start | bytes 12582916 | tf_op jit(solution)/shard_map/while
  146.9 3.6 %copy-start = (f32[2048,256,2]{1,0,2:T(8,128)S(1)}, f32[2048,256,2]{1,0,2:T(8,128)}, u32[]{:S(2)}) copy-start(f32[2048,256,2]{1,0,2:T(8,128)} %get-tuple-element.177) | copy-start | bytes 12582916 | tf_op jit(solution)/shard_map/while
  155.4 3.6 %copy-start = (f32[2048,256,2]{1,0,2:T(8,128)S(1)}, f32[2048,256,2]{1,0,2:T(8,128)}, u32[]{:S(2)}) copy-start(f32[2048,256,2]{1,0,2:T(8,128)} %get-tuple-element.177) | copy-start | bytes 12582916 | tf_op jit(solution)/shard_map/while
  163.5 3.9 %copy-start = (f32[2048,256,2]{1,0,2:T(8,128)S(1)}, f32[2048,256,2]{1,0,2:T(8,128)}, u32[]{:S(2)}) copy-start(f32[2048,256,2]{1,0,2:T(8,128)} %get-tuple-element.177) | copy-start | bytes 12582916 | tf_op jit(solution)/shard_map/while
  172.0 4.1 %copy-start = (f32[2048,256,2]{1,0,2:T(8,128)S(1)}, f32[2048,256,2]{1,0,2:T(8,128)}, u32[]{:S(2)}) copy-start(f32[2048,256,2]{1,0,2:T(8,128)} %get-tuple-element.177) | copy-start | bytes 12582916 | tf_op jit(solution)/shard_map/while
  180.5 3.8 %copy-start = (f32[2048,256,2]{1,0,2:T(8,128)S(1)}, f32[2048,256,2]{1,0,2:T(8,128)}, u32[]{:S(2)}) copy-start(f32[2048,256,2]{1,0,2:T(8,128)} %get-tuple-element.177) | copy-start | bytes 12582916 | tf_op jit(solution)/shard_map/while
  185.1 12.6 %copy-start.2 = (f32[2048]{0:T(1024)S(1)}, f32[2048]{0:T(1024)}, u32[]{:S(2)}) copy-start(f32[2048]{0:T(1024)} %param.23) | copy-start | bytes 24580
  185.1 12.6 %copy-start.3 = (f32[2048]{0:T(1024)S(1)}, f32[2048]{0:T(1024)}, u32[]{:S(2)}) copy-start(f32[2048]{0:T(1024)} %param.22) | copy-start | bytes 24580
  224.2 15.9 %copy-start.4 = (f32[2048]{0:T(1024)S(1)}, f32[2048]{0:T(1024)}, u32[]{:S(2)}) copy-start(f32[2048]{0:T(1024)} %param.27) | copy-start | bytes 24580
  224.2 15.9 %copy-start.5 = (f32[2048]{0:T(1024)S(1)}, f32[2048]{0:T(1024)}, u32[]{:S(2)}) copy-start(f32[2048]{0:T(1024)} %param.26) | copy-start | bytes 24580
Sparse Core Ops, SparseCore 0:
  11.0 89.1 all-gather.2
  103.0 99.6 all-gather.4
where the time goes:
time: 252 us; the launch traced here: 248 us
  waiting for transfers between devices  83.4 us (33%)
  matrix products  70.9 us (28%)
  blocking collectives  39.7 us (16%)
  local copies, waits for them, and re-layouts  24.8 us (10%)
  other arithmetic  15.1 us (6%)
  between operations  13.8 us (5%)
    all_gather x2, waiting for transfers between devices, side_by_side(): lax.all_gather(both, axis, axis=dim, tiled=True)  83.3 us
    dot_general x8, matrix products, advance(): jnp.einsum('qkgd,skd->kgqs', query_grp, key_block, preferred_element_type...  30.5 us
    dot_general x8, matrix products, advance(): jnp.einsum('kgqs,skd->kgqd', weights.astype(jnp.bfloat16), value_block, p...  27 us
    all_to_all x1, blocking collectives, sent_to_all(): return lax.all_to_all(copies, axis, split_axis=0, concat_axis=0, tiled=True)  15.9 us
    all_to_all x1, blocking collectives, sum_at_owner(): lax.all_to_all(parts, axis, split_axis=0, concat_axis=0, tiled=True)  15.1 us
    unnamed x16, local copies, waits for them, and re-layouts  13.9 us
    dot_general x1, matrix products, per_device(): lax.dot_general(hidden, whole_down, (((1,), (1,)), ((), ())), preferred_e...  10.3 us
    all_to_all x1, blocking collectives, per_device(): lax.all_to_all(attended, 'tp', split_axis=0, concat_axis=1, tiled=True)  8.73 us
  transfers between devices with their start and end apart: 2, of which 1 were waited for; matrix products, arithmetic and copies ran while one was open for 37% of the time, Pallas kernels for 0%

commit v1 on v0

v1 whole, which is shorter than its diff:
```python
import functools

import jax
import jax.numpy as jnp
import numpy as np
from jax import lax
from jax.experimental import pallas as pl
from jax.experimental.pallas import tpu as pltpu
from jax.sharding import PartitionSpec as P

MESH = pl.DeviceIdType.MESH
HEAD_DIM = 128
GRID_W = 64
RESIDUAL_SCALE = 2.0**0.25
LAYER_EPS = 1e-05
HEAD_EPS = 1e-06
ROTARY_BASE = 10000.0
NZ, NX, NC, NY = 8, 4, 2, 4
SCALE2 = float(np.log2(np.e) * HEAD_DIM**-0.5)
AW = 640
W_COLS = 1024
PASS1 = 3 * 512
KEYS = 4096
F32, BF16 = jnp.float32, jnp.bfloat16


def rotary_tables():
    inverse = (np.float32(ROTARY_BASE) ** (-np.arange(32, dtype=np.float32) / np.float32(32))).astype(np.float32)
    ang = np.arange(256, dtype=np.float32)[:, None] * inverse
    sign = np.tile(np.array([-1.0, 1.0], np.float32), 32)
    cos = np.repeat(np.cos(ang), 2, axis=1).astype(np.float32)
    sin = np.repeat(np.sin(ang), 2, axis=1).astype(np.float32) * sign
    return cos, sin


class Copy:
    def __init__(self, pool, src, dst, land, dev):
        self.n = pool.take()
        self.pool, self.src, self.dst, self.land, self.dev = pool, src, dst, land, dev

    def start(self):
        self._make(self.src(), self.dst()).start()

    def wait(self):
        here = self.land()
        self._make(here, here).wait_recv()

    def drain(self):
        src = self.src()
        self._make(src, self.dst()).wait_send()

    def _make(self, src, dst):
        return pltpu.make_async_remote_copy(
            src_ref=src, dst_ref=dst, send_sem=self.pool.ssem.at[self.n], recv_sem=self.pool.rsem.at[self.n],
            device_id=self.dev, device_id_type=MESH,
        )


class Pool:
    def __init__(self, ssem, rsem, size):
        self.ssem, self.rsem, self.size, self.n, self.all = ssem, rsem, size, 0, []

    def take(self):
        self.n += 1
        assert self.n <= self.size
        return self.n - 1

    def copy(self, src, dst, land, dev):
        c = Copy(self, src, dst, land, dev)
        self.all.append(c)
        return c


N_SEMS = 192


def layer_norm(summed, gain, bias):
    centred = summed - jnp.mean(summed, axis=-1, keepdims=True)
    variance = jnp.mean(centred * centred, axis=-1, keepdims=True)
    return centred * lax.rsqrt(variance + LAYER_EPS) * gain + bias


def norm_rotate(x, gain, cos, sin):
    x = x.astype(F32)
    x = x * lax.rsqrt(jnp.mean(x * x, axis=-1, keepdims=True) + HEAD_EPS) * gain
    even = lax.broadcasted_iota(jnp.int32, x.shape, 1) % 2 == 0
    swapped = jnp.where(even, pltpu.roll(x, HEAD_DIM - 1, 1), pltpu.roll(x, 1, 1))
    return (x * cos + swapped * sin).astype(BF16)


def eye128():
    return lax.broadcasted_iota(jnp.int32, (128, 128), 0) == lax.broadcasted_iota(jnp.int32, (128, 128), 1)


def dot(a, b, dims=((1,), (0,))):
    return lax.dot_general(a, b, (dims, ((), ())), preferred_element_type=F32)


def kernel(
    q_ref, k_ref, v_ref, cos_ref, sin_ref, qg_ref, kg_ref, fg_ref, fb_ref, sg_ref, sb_ref,
    res_hbm, ow_hbm, up_hbm, dn_hbm,
    out_ref,
    kvbuf, qbuf, o_acc, m_acc, l_acc, s_scr, osend, orecv, stsend, strecv, att_s, attbuf, ow, res, xbuf,
    upbuf, dnbuf, hid, psend, precv, pown, ysend, yrecv, fin,
    ssem, rsem, lsem,
):
    sp, y = lax.axis_index("sp"), lax.axis_index("tp")
    z, x, c = sp // 8, (sp // 2) % 4, sp % 2
    pool = Pool(ssem, rsem, N_SEMS)

    def dev(dz=0, dx=0, dy=0, flip=False):
        zz, xx, yy = (z + dz + NZ) % NZ, (x + dx + NX) % NX, (y + dy + NY) % NY
        cc = 1 - c if flip else c
        return (zz * 8 + xx * 2 + cc, yy)

    def zat(d):
        return (z + d + NZ) % NZ

    def xat(d):
        return (x + d + NX) % NX

    barrier = pltpu.get_barrier_semaphore()
    partners = [dict(dz=1), dict(dz=-1), dict(dx=1), dict(dx=-1), dict(dx=2), dict(dy=1), dict(dy=-1), dict(dy=2), dict(flip=True)]
    for p in partners:
        pl.semaphore_signal(barrier, inc=1, device_id=dev(**p), device_id_type=MESH)

    def block(zs, xs):
        return pl.multiple_of(zs * 256 + xs * 64, 64)

    mine = pl.multiple_of(c * W_COLS, W_COLS)
    other = pl.multiple_of((1 - c) * W_COLS, W_COLS)
    my_rows = pl.ds(pl.multiple_of(block(z, x) + c * 32, 32), 32)
    partner_rows = pl.ds(pl.multiple_of(block(z, x) + (1 - c) * 32, 32), 32)
    local = [
        pltpu.make_async_copy(up_hbm.at[:, pl.ds(mine, W_COLS)], upbuf.at[my_rows, :], lsem.at[0]),
        pltpu.make_async_copy(dn_hbm.at[:, pl.ds(mine, W_COLS)], dnbuf.at[my_rows, :], lsem.at[1]),
        pltpu.make_async_copy(ow_hbm, ow, lsem.at[2]),
        pltpu.make_async_copy(res_hbm, res, lsem.at[3]),
    ]
    for l in local:
        l.start()

    cos, sin = cos_ref[...], sin_ref[...]
    kvbuf[0:256, 0:128] = norm_rotate(k_ref[...], kg_ref[...], cos, sin)
    kvbuf[0:256, 128:256] = v_ref[...]
    qbuf[0:256, :] = norm_rotate(q_ref[:, 0:128], qg_ref[...], cos, sin)
    qbuf[256:512, :] = norm_rotate(q_ref[:, 128:256], qg_ref[...], cos, sin)

    def same(ref, rows, cols, land_rows, device):
        view = lambda: ref.at[pl.ds(*rows), pl.ds(*cols)]
        return pool.copy(view, view, lambda: ref.at[pl.ds(*land_rows), pl.ds(*cols)], device)

    flip = dev(flip=True)
    KP, KM, KD = {}, {}, {}
    full = (0, 256)
    for s in range(1, 5):
        lo, n = (0, 256) if s < 4 else (0, 128)
        src = 0 if s == 1 else 2 * (s - 1) - 1
        dst = 2 * s - 1
        KP[s] = pool.copy(
            lambda src=src, lo=lo, n=n: kvbuf.at[pl.ds(src * 512 + lo, n), :],
            lambda dst=dst, lo=lo, n=n: kvbuf.at[pl.ds(dst * 512 + lo, n), :],
            lambda dst=dst, lo=lo, n=n: kvbuf.at[pl.ds(dst * 512 + lo, n), :], dev(dz=1))
        lo = 0 if s < 4 else 128
        src = 0 if s == 1 else 2 * (s - 1)
        dst = 2 * s if s < 4 else 7
        KM[s] = pool.copy(
            lambda src=src, lo=lo, n=n: kvbuf.at[pl.ds(src * 512 + lo, n), :],
            lambda dst=dst, lo=lo, n=n: kvbuf.at[pl.ds(dst * 512 + lo, n), :],
            lambda dst=dst, lo=lo, n=n: kvbuf.at[pl.ds(dst * 512 + lo, n), :], dev(dz=-1))
    for j in range(8):
        KD[j] = pool.copy(
            lambda j=j: kvbuf.at[pl.ds(j * 512, 256), :],
            lambda j=j: kvbuf.at[pl.ds(j * 512 + 256, 256), :],
            lambda j=j: kvbuf.at[pl.ds(j * 512 + 256, 256), :], flip)
    QS, OS, ST, AT = {}, {}, {}, {}
    for d in range(1, 4):
        QS[d] = pool.copy(
            lambda: qbuf.at[pl.ds(0, 512), :], lambda d=d: qbuf.at[pl.ds(d * 512, 512), :],
            lambda d=d: qbuf.at[pl.ds(d * 512, 512), :], dev(dx=d))
        OS[d] = pool.copy(lambda d=d: osend.at[d], lambda d=d: orecv.at[d], lambda d=d: orecv.at[d], dev(dx=-d))
        ST[d] = pool.copy(lambda d=d: stsend.at[d], lambda d=d: strecv.at[d], lambda d=d: strecv.at[d], dev(dx=-d))
        AT[d] = pool.copy(
            lambda d=d: att_s.at[pl.ds(pl.multiple_of((y + d) % NY * 64, 64), 64), :],
            lambda d=d: attbuf.at[d], lambda d=d: attbuf.at[d], dev(dy=d))
    def rows_of(ref, lo, n):
        return lambda: ref.at[pl.ds(lo, n), :]

    YP1 = pool.copy(rows_of(xbuf, 0, 64), rows_of(xbuf, 64, 64), rows_of(xbuf, 64, 64), dev(dy=1))
    YM1 = pool.copy(rows_of(xbuf, 0, 64), rows_of(xbuf, 192, 64), rows_of(xbuf, 192, 64), dev(dy=-1))
    YP2 = pool.copy(rows_of(xbuf, 64, 32), rows_of(xbuf, 128, 32), rows_of(xbuf, 128, 32), dev(dy=1))
    YM2 = pool.copy(rows_of(xbuf, 224, 32), rows_of(xbuf, 160, 32), rows_of(xbuf, 160, 32), dev(dy=-1))
    XD = [pool.copy(rows_of(xbuf, j * 64, 64), rows_of(xbuf, 256 + j * 64, 64), rows_of(xbuf, 256 + j * 64, 64), flip) for j in range(4)]

    def exchange(hbm, buf):
        return pool.copy(
            lambda: hbm.at[:, pl.ds(other, W_COLS)], lambda: buf.at[my_rows, :], lambda: buf.at[partner_rows, :], flip)

    WX = {"u": exchange(up_hbm, upbuf), "d": exchange(dn_hbm, dnbuf)}
    order = [0, -1, 1, -2, 2, -3, 3, 4]

    class Gather:
        def __init__(self, buf):
            a, b = (0, AW), (AW, W_COLS - AW)
            up, down, right, left = dev(dz=1), dev(dz=-1), dev(dx=1), dev(dx=-1)
            self.AP, self.AM, self.BP, self.BM = {}, {}, {}, {}
            for s in range(1, 5):
                n, m = (64, 256) if s < 4 else (32, 128)
                h, g = (0, 0) if s < 4 else (32, 128)
                self.AP[s] = same(buf, (block(zat(1 - s), x), n), a, (block(zat(-s), x), n), up)
                self.AM[s] = same(buf, (block(zat(s - 1), x) + h, n), a, (block(zat(s), x) + h, n), down)
                self.BP[s] = same(buf, (block(zat(1 - s), 0), m), b, (block(zat(-s), 0), m), up)
                self.BM[s] = same(buf, (block(zat(s - 1), 0) + g, m), b, (block(zat(s), 0) + g, m), down)
            self.ax = {d: self.spread(buf, zat(d), a, right, left) for d in order}
            self.bx = self.spread(buf, z, b, right, left)

        def spread(self, buf, zs, cols, right, left):
            return (
                same(buf, (block(zs, x), 64), cols, (block(zs, xat(-1)), 64), right),
                same(buf, (block(zs, x), 64), cols, (block(zs, xat(1)), 64), left),
                same(buf, (block(zs, xat(-1)), 32), cols, (block(zs, xat(-2)), 32), right),
                same(buf, (block(zs, xat(1)) + 32, 32), cols, (block(zs, xat(2)) + 32, 32), left),
            )

        def begin(self):
            for t in (self.bx[0], self.bx[1], self.AP[1], self.AM[1], self.ax[0][0], self.ax[0][1]):
                t.start()

        def pass_on(self, sp4):
            sp4[0].wait()
            sp4[2].start()
            sp4[1].wait()
            sp4[3].start()

        def first_x(self):
            self.pass_on(self.bx)
            self.pass_on(self.ax[0])

        def row(self):
            self.bx[2].wait()
            self.bx[3].wait()
            self.BP[1].start()
            self.BM[1].start()

        def a_step(self, s):
            self.AP[s].wait()
            if s < 4:
                self.AP[s + 1].start()
            self.AM[s].wait()
            if s < 4:
                self.AM[s + 1].start()
            for d in (-s, s) if s < 4 else (4,):
                self.ax[d][0].start()
                self.ax[d][1].start()

        def b_step(self, s):
            self.BP[s].wait()
            if s < 4:
                self.BP[s + 1].start()
            self.BM[s].wait()
            if s < 4:
                self.BM[s + 1].start()

        def x_step(self, s):
            for d in (-s, s) if s < 4 else (4,):
                self.pass_on(self.ax[d])

        def have(self, d):
            self.ax[d][2].wait()
            self.ax[d][3].wait()

        def events(self):
            steps = [self.begin, self.first_x, self.row]
            for s in range(1, 4):
                steps += [functools.partial(self.a_step, s), functools.partial(self.b_step, s), functools.partial(self.x_step, s)]
            return steps + [functools.partial(self.a_step, 4), functools.partial(self.b_step, 4), functools.partial(self.x_step, 4)]

    U, D = Gather(upbuf), Gather(dnbuf)
    DD = [pool.copy(lambda j=j: psend.at[j], lambda j=j: precv.at[j], lambda j=j: precv.at[j], flip) for j in range(8)]
    RS = [
        [pool.copy(lambda j=j, k=k: ysend.at[j, k], lambda j=j, k=k: yrecv.at[j, k], lambda j=j, k=k: yrecv.at[j, k], dev(dy=-k)) for k in (1, 2, 3)]
        for j in range(8)
    ]

    u, d = U.events(), D.events()
    queue = u[0:6] + [d[0]] + u[6:9] + d[1:3] + u[9:12] + d[3:6] + u[12:15] + d[6:15]
    at = [0]

    def w(n):
        for e in queue[at[0] : at[0] + n]:
            e()
        at[0] += n

    pl.semaphore_wait(barrier, len(partners))
    KP[1].start()
    KM[1].start()
    KD[0].start()
    for i in (1, 3, 2):
        QS[i].start()
    WX["u"].start()
    WX["d"].start()
    local[0].wait()
    WX["u"].wait()
    w(1)
    local[1].wait()
    WX["d"].wait()
    KP[1].wait()
    KP[2].start()
    KD[1].start()
    KM[1].wait()
    KM[2].start()
    KD[2].start()
    for i in range(3):
        KD[i].wait()
    w(1)
    for i in (1, 2, 3):
        QS[i].wait()

    def kv_step(s):
        KP[s].wait()
        KM[s].wait()
        if s < 4:
            KP[s + 1].start()
            KM[s + 1].start()
            KD[2 * s - 1].start()
            KD[2 * s].start()
        else:
            KD[7].start()

    def scores(row, lo, hi):
        q = qbuf[pl.ds(row, 256), :]
        best = None
        for at_key in range(lo, hi, 512):
            part = dot(q, kvbuf[pl.ds(at_key, 512), 0:128], ((1,), (1,)))
            s_scr[:, pl.ds(at_key - lo, 512)] = part
            for g in range(0, 512, 128):
                best = part[:, g : g + 128] if best is None else jnp.maximum(best, part[:, g : g + 128])
        return jnp.max(best, axis=1, keepdims=True)

    def weigh(m, lo, hi):
        total, out = None, None
        for at_key in range(lo, hi, 512):
            p = jnp.exp2((s_scr[:, pl.ds(at_key - lo, 512)] - m) * SCALE2)
            for g in range(0, 512, 128):
                total = p[:, g : g + 128] if total is None else total + p[:, g : g + 128]
            o = dot(p.astype(BF16), kvbuf[pl.ds(at_key, 512), 128:256])
            out = o if out is None else out + o
        return jnp.sum(total, axis=1, keepdims=True), out

    def events_at(i, table):
        for step, fns in table.items():
            @pl.when(i == step)
            def _(fns=fns):
                for f in fns:
                    f()

    def pass1(i, _):
        row = pl.multiple_of((i + 2) % 8 * 256, 256)
        m = scores(row, 0, PASS1)
        l, o = weigh(m, 0, PASS1)
        o_acc[pl.ds(row, 256), :] = o
        m_acc[pl.ds(row, 256), :] = jnp.broadcast_to(m, (256, 128))
        l_acc[pl.ds(row, 256), :] = jnp.broadcast_to(l, (256, 128))
        events_at(i, ev1)
        return 0

    def grab(n):
        got = queue[at[0] : at[0] + n]
        at[0] += n
        return got

    ev1 = {1: [lambda: kv_step(2)], 2: grab(1), 4: [lambda: kv_step(3)] + grab(1), 6: grab(1), 7: grab(1) + [lambda: kv_step(4)]}
    lax.fori_loop(0, 8, pass1, 0)
    for i in range(3, 8):
        KD[i].wait()

    def send_o(d):
        eye = eye128()
        for g in range(4):
            rows = pl.ds(d * 512 + g * 128, 128)
            stsend[d, g : g + 1, :] = jnp.sum(jnp.where(eye, m_acc[rows, :], 0.0), axis=0, keepdims=True)
            stsend[d, g + 4 : g + 5, :] = jnp.sum(jnp.where(eye, l_acc[rows, :], 0.0), axis=0, keepdims=True)
        OS[d].start()
        ST[d].start()

    def pass2(i, _):
        row = pl.multiple_of((i + 2) % 8 * 256, 256)
        m_old = m_acc[pl.ds(row, 256), 0:1]
        m = jnp.maximum(scores(row, PASS1, KEYS), m_old)
        alpha = jnp.exp2((m_old - m) * SCALE2)
        l, o = weigh(m, PASS1, KEYS)
        o = o_acc[pl.ds(row, 256), :] * alpha + o
        l = l_acc[pl.ds(row, 256), 0:1] * alpha + l
        o_acc[pl.ds(row, 256), :] = o
        m_acc[pl.ds(row, 256), :] = jnp.broadcast_to(m, (256, 128))
        l_acc[pl.ds(row, 256), :] = jnp.broadcast_to(l, (256, 128))
        osend[row // 512, pl.ds(pl.multiple_of(row % 512, 256), 256), :] = o.astype(BF16)
        events_at(i, ev2)
        return 0

    ev2 = {
        0: grab(1), 1: [lambda: send_o(1)], 2: grab(1), 3: [lambda: send_o(2)] + grab(1), 4: grab(1), 5: [lambda: send_o(3)], 6: grab(1), 7: grab(1),
    }
    lax.fori_loop(0, 8, pass2, 0)

    for i in (1, 2, 3):
        ST[i].wait()
    for i in (1, 2, 3):
        OS[i].wait()
    eye = eye128()
    for g in range(4):
        rows = pl.ds(g * 128, 128)
        ms, ls = [m_acc[rows, 0:1]], [l_acc[rows, 0:1]]
        for i in (1, 2, 3):
            ms.append(jnp.sum(jnp.where(eye, strecv[i, g : g + 1, :], 0.0), axis=1, keepdims=True))
            ls.append(jnp.sum(jnp.where(eye, strecv[i, g + 4 : g + 5, :], 0.0), axis=1, keepdims=True))
        top = jnp.maximum(jnp.maximum(ms[0], ms[1]), jnp.maximum(ms[2], ms[3]))
        es = [jnp.exp2((m - top) * SCALE2) for m in ms]
        num = o_acc[rows, :] * es[0]
        den = ls[0] * es[0]
        for i in (1, 2, 3):
            num += orecv[i, g * 128 : g * 128 + 128, :].astype(F32) * es[i]
            den += ls[i] * es[i]
        att_s[(g % 2) * 128 : (g % 2) * 128 + 128, (g // 2) * 128 : (g // 2) * 128 + 128] = (num / den).astype(BF16)
    for i in (1, 3, 2):
        AT[i].start()
    local[2].wait()
    local[3].wait()
    w(1)
    for i in (1, 2, 3):
        AT[i].wait()
    mixed = RESIDUAL_SCALE * res[...].astype(F32)
    for i in range(4):
        a = att_s[pl.ds(pl.multiple_of(y * 64, 64), 64), :] if i == 0 else attbuf[i]
        mixed += dot(a, ow[pl.ds(pl.multiple_of((y - i + NY) % NY * 256, 256), 256), :])
    xbuf[0:64, :] = layer_norm(mixed, fg_ref[...], fb_ref[...]).astype(BF16)
    YP1.start()
    YM1.start()
    XD[0].start()
    w(2)
    YP1.wait()
    YP2.start()
    XD[1].start()
    YM1.wait()
    YM2.start()
    XD[3].start()
    w(2)
    YP2.wait()
    YM2.wait()
    XD[2].start()
    w(2)
    for i in range(4):
        XD[i].wait()

    u_left = [f for f in u if f in queue[at[0] :]]
    while any(f in queue[at[0] :] for f in u_left):
        w(1)
    for i in order:
        U.have(i)

    def up_tile(i, _):
        cols = pl.ds(pl.multiple_of(i * 256, 256), 256)
        h = jnp.maximum(dot(xbuf[...], upbuf[:, cols]), 0.0)
        hid[:, cols] = (h * h).astype(BF16)
        return 0

    lax.fori_loop(0, 4, up_tile, 0)

    def combine(j, zs):
        DD[j].wait()
        cols = pl.ds(pl.multiple_of(zs * 256, 256), 256)
        both = pown[j % 2] + precv[j].astype(F32)
        fin[:, cols] = both[0:64]
        for k in (1, 2, 3):
            ysend[j, k] = both[k * 64 : k * 64 + 64].astype(BF16)
        for k in (1, 3, 2):
            RS[j][k - 1].start()

    need = {0: d.index(d[5]) + 1, 1: 6, 2: 6, 3: 9, 4: 9, 5: 12, 6: 12, 7: 15}
    done_d = [len([f for f in d if f not in queue[at[0] :]])]
    need[0] = 3
    for j, dz in enumerate(order):
        while done_d[0] < need[j]:
            d[done_d[0]]()
            done_d[0] += 1
        D.have(dz)
        zs = zat(dz)
        part = dot(hid[...], dnbuf[pl.ds(pl.multiple_of(zs * 256, 256), 256), :], ((1,), (1,)))
        pown[j % 2] = part[0:256]
        psend[j] = part[256:512].astype(BF16)
        DD[j].start()
        if j > 0:
            combine(j - 1, zat(order[j - 1]))
    combine(7, zat(4))

    for j, dz in enumerate(order):
        cols = pl.ds(pl.multiple_of(zat(dz) * 256, 256), 256)
        for k in (1, 2, 3):
            RS[j][k - 1].wait()
        fin[:, cols] = fin[:, cols] + (yrecv[j, 1].astype(F32) + yrecv[j, 2].astype(F32) + yrecv[j, 3].astype(F32))
    summed = RESIDUAL_SCALE * xbuf[0:64, :].astype(F32) + fin[...]
    out_ref[...] = layer_norm(summed, sg_ref[...], sb_ref[...]).astype(BF16)
    for t in pool.all:
        t.drain()


def per_device(
    queries, keys, values, residual, query_gain, key_gain, out_weight, first_gain, first_bias, up_weight, down_weight,
    second_gain, second_bias,
):
    cos, sin = rotary_tables()
    sp = lax.axis_index("sp")

    def table(t):
        t = jnp.asarray(t)
        row = jnp.broadcast_to(lax.dynamic_slice_in_dim(t, sp * 4, 4, 0)[:, None, :], (4, GRID_W, 64))
        col = jnp.broadcast_to(t[None, :GRID_W, :], (4, GRID_W, 64))
        return jnp.concatenate([row, col], axis=-1).reshape(256, HEAD_DIM)

    vmem, hbm = pl.BlockSpec(memory_space=pltpu.VMEM), pl.BlockSpec(memory_space=pl.ANY)
    scratch = [
        pltpu.VMEM((KEYS, 256), BF16),
        pltpu.VMEM((2048, 128), BF16),
        pltpu.VMEM((2048, 128), F32),
        pltpu.VMEM((2048, 128), F32),
        pltpu.VMEM((2048, 128), F32),
        pltpu.VMEM((256, KEYS - PASS1), F32),
        pltpu.VMEM((4, 512, 128), BF16),
        pltpu.VMEM((4, 512, 128), BF16),
        pltpu.VMEM((4, 8, 128), F32),
        pltpu.VMEM((4, 8, 128), F32),
        pltpu.VMEM((256, 256), BF16),
        pltpu.VMEM((4, 64, 256), BF16),
        pltpu.VMEM((1024, 2048), BF16),
        pltpu.VMEM((64, 2048), BF16),
        pltpu.VMEM((512, 2048), BF16),
        pltpu.VMEM((2048, W_COLS), BF16),
        pltpu.VMEM((2048, W_COLS), BF16),
        pltpu.VMEM((512, W_COLS), BF16),
        pltpu.VMEM((8, 256, 256), BF16),
        pltpu.VMEM((8, 256, 256), BF16),
        pltpu.VMEM((2, 256, 256), F32),
        pltpu.VMEM((8, 4, 64, 256), BF16),
        pltpu.VMEM((8, 4, 64, 256), BF16),
        pltpu.VMEM((64, 2048), F32),
        pltpu.SemaphoreType.DMA((N_SEMS,)),
        pltpu.SemaphoreType.DMA((N_SEMS,)),
        pltpu.SemaphoreType.DMA((4,)),
    ]
    return pl.pallas_call(
        kernel,
        out_shape=jax.ShapeDtypeStruct((64, 2048), BF16),
        in_specs=[vmem] * 11 + [hbm] * 4,
        out_specs=vmem,
        scratch_shapes=scratch,
        compiler_params=pltpu.CompilerParams(collective_id=0, has_side_effects=True, vmem_limit_bytes=62 * 1024 * 1024),
        name="layer",
    )(
        queries, keys, values, table(cos), table(sin), query_gain[None], key_gain[None], first_gain[None], first_bias[None],
        second_gain[None], second_bias[None], residual, out_weight, up_weight, down_weight,
    )


def solution(mesh):
    in_specs = (
        P("sp", "tp"), P("sp", "tp"), P("sp", "tp"), P(("sp", "tp"), None), P(), P(), P(), P(), P(),
        P("sp", "tp"), P("sp", "tp"), P(), P(),
    )
    return jax.shard_map(per_device, mesh=mesh, in_specs=in_specs, out_specs=P(("sp", "tp"), None), check_vma=False)
```

time: 252 us -> 132 us (0.52); the launches traced: 248 us -> 132 us
  Pallas kernels: 0 us -> 126 us
  waiting for transfers between devices: 83.4 us -> 0 us
  matrix products: 70.9 us -> 0 us
  blocking collectives: 39.7 us -> 0 us
  local copies, waits for them, and re-layouts: 24.8 us -> 3.94 us
  between operations: 13.8 us -> 0.03 us
  other arithmetic: 15.1 us -> 1.52 us
    pallas_call x0 -> x1, Pallas kernels: none -> 126 us  [per_device(): pl.pallas_call(kernel, out_shape=jax.ShapeDtypeStruct((64, 2048), BF16),...]
    all_gather x2 -> x0, waiting for transfers between devices: 83.3 us -> none  [side_by_side(): lax.all_gather(both, axis, axis=dim, tiled=True)]
    dot_general x18 -> x0, matrix products: 70.9 us -> none  [the longest x8 30.5 us: advance(): jnp.einsum('qkgd,skd->kgqs', query_grp, key_block, preferred_element_type...]
    all_to_all x3 -> x0, blocking collectives: 39.7 us -> none  [the longest x1 15.9 us: sent_to_all(): return lax.all_to_all(copies, axis, split_axis=0, concat_axis=0, tiled=True)]
    unnamed x16 -> x1, local copies, waits for them, and re-layouts: 13.9 us -> 1.67 us
    reduce_sum x14 -> x0, other arithmetic: 7.89 us -> none  [the longest x8 5.6 us: advance(): total = total * factor + jnp.sum(weights, axis=-1)]
    slice x2 -> x0, local copies, waits for them, and re-layouts: 5.9 us -> none  [the longest x1 5.79 us: side_by_side(): lax.slice_in_dim(result, at, at + a.shape[along], axis=along)]
    while x24 -> x0, local copies, waits for them, and re-layouts: 2.74 us -> none
  transfers between devices with their start and end apart: 2 -> 0, of which waited for: 1 -> 0; matrix products, arithmetic and copies ran while one was open for 37% -> 0% of each run, Pallas kernels for 0% -> 0%
where the time goes in v1:
time: 132 us
  Pallas kernels  126 us (95%)
  local copies, waits for them, and re-layouts  3.94 us (3%)
  other arithmetic  1.52 us (1%)
    pallas_call x1, Pallas kernels, per_device(): pl.pallas_call(kernel, out_shape=jax.ShapeDtypeStruct((64, 2048), BF16),...  126 us

profile of v1, /device:TPU:1, one launch (start us, length us, event | category | flops | bytes accessed | tf_op | source)
XLA Modules:
  0.0 131.5 jit_solution(14968525704891366959)
XLA Ops:
  0.0 0.7 constant_dynamic-slice_fusion
  0.7 0.8 broadcast_in_dim.21
  1.5 0.8 pad_maximum_fusion
  2.3 0.8 broadcast_in_dim.45
  3.0 0.8 pad_maximum_fusion.1
  3.8 126.0 %layer.1 = bf16[64,2048]{1,0:T(8,128)(2,1)} custom-call(bf16[256,256]{1,0:T(8,128)(2,1)} %q_ref.1, bf16[256,128]{1,0:T(8,128)(2,1)} %k_ref.1, bf16[256,128]{1,0:T(8,128)(2,1)} %v_ref.1, f32[256,128]{1,0:T(8,128)} %bitcast.8, f32[256,128]{1,0:T(8,128)} %bitcast.9, f32[1,128]{1,0:T(1,128)} %bitcast.14, f32[1,128]{1,0:T(1,128)} %bitcast.15, ...), custom_call_target="tpu_custom_call" | custom-call | tf_op jit(solution)/shard_map/layer/pallas_call | solution.py:550
  129.9 1.7 %copy.17 = bf16[64,2048]{1,0:T(8,128)(2,1)} copy(bf16[64,2048]{1,0:T(8,128)(2,1)} %layer.1) | data formatting | bytes 524288
  (2 shorter events, 0.0 us)

commit v2 on v1

--- a/solution.py
+++ b/solution.py
@@ -56,6 +56,18 @@
         )
 
 
+class Phases:
+    def __init__(self):
+        self.scope = None
+
+    def __call__(self, name):
+        if self.scope is not None:
+            self.scope.__exit__(None, None, None)
+        self.scope = jax.named_scope(name) if name else None
+        if name:
+            self.scope.__enter__()
+
+
 class Pool:
     def __init__(self, ssem, rsem, size):
         self.ssem, self.rsem, self.size, self.n, self.all = ssem, rsem, size, 0, []
@@ -71,7 +83,7 @@
         return c
 
 
-N_SEMS = 192
+N_SEMS = 240
 
 
 def layer_norm(summed, gain, bias):
@@ -97,7 +109,7 @@
 
 
 def kernel(
-    q_ref, k_ref, v_ref, cos_ref, sin_ref, qg_ref, kg_ref, fg_ref, fb_ref, sg_ref, sb_ref,
+    q_ref, k_ref, v_ref, cosr_ref, cosc_ref, sinr_ref, sinc_ref, qg_ref, kg_ref, fg_ref, fb_ref, sg_ref, sb_ref,
     res_hbm, ow_hbm, up_hbm, dn_hbm,
     out_ref,
     kvbuf, qbuf, o_acc, m_acc, l_acc, s_scr, osend, orecv, stsend, strecv, att_s, attbuf, ow, res, xbuf,
@@ -107,6 +119,8 @@
     sp, y = lax.axis_index("sp"), lax.axis_index("tp")
     z, x, c = sp // 8, (sp // 2) % 4, sp % 2
     pool = Pool(ssem, rsem, N_SEMS)
+    phase = Phases()
+    phase("p_prep")
 
     def dev(dz=0, dx=0, dy=0, flip=False):
         zz, xx, yy = (z + dz + NZ) % NZ, (x + dx + NX) % NX, (y + dy + NY) % NY
@@ -140,7 +154,12 @@
     for l in local:
         l.start()
 
-    cos, sin = cos_ref[...], sin_ref[...]
+    def angles(rows, cols):
+        cols = cols[...]
+        parts = [jnp.broadcast_to(rows[pl.ds(sp * 4 + i, 1), :], (GRID_W, HEAD_DIM)) + cols for i in range(4)]
+        return jnp.concatenate(parts, axis=0)
+
+    cos, sin = angles(cosr_ref, cosc_ref), angles(sinr_ref, sinc_ref)
     kvbuf[0:256, 0:128] = norm_rotate(k_ref[...], kg_ref[...], cos, sin)
     kvbuf[0:256, 128:256] = v_ref[...]
     qbuf[0:256, :] = norm_rotate(q_ref[:, 0:128], qg_ref[...], cos, sin)
@@ -152,22 +171,17 @@
 
     flip = dev(flip=True)
     KP, KM, KD = {}, {}, {}
-    full = (0, 256)
+
+    def ring(src, dst, lo, device):
+        view = lambda slot: kvbuf.at[pl.ds(slot * 512 + lo, 128), :]
+        return pool.copy(lambda: view(src), lambda: view(dst), lambda: view(dst), device)
+
     for s in range(1, 5):
-        lo, n = (0, 256) if s < 4 else (0, 128)
-        src = 0 if s == 1 else 2 * (s - 1) - 1
-        dst = 2 * s - 1
-        KP[s] = pool.copy(
-            lambda src=src, lo=lo, n=n: kvbuf.at[pl.ds(src * 512 + lo, n), :],
-            lambda dst=dst, lo=lo, n=n: kvbuf.at[pl.ds(dst * 512 + lo, n), :],
-            lambda dst=dst, lo=lo, n=n: kvbuf.at[pl.ds(dst * 512 + lo, n), :], dev(dz=1))
-        lo = 0 if s < 4 else 128
-        src = 0 if s == 1 else 2 * (s - 1)
-        dst = 2 * s if s < 4 else 7
-        KM[s] = pool.copy(
-            lambda src=src, lo=lo, n=n: kvbuf.at[pl.ds(src * 512 + lo, n), :],
-            lambda dst=dst, lo=lo, n=n: kvbuf.at[pl.ds(dst * 512 + lo, n), :],
-            lambda dst=dst, lo=lo, n=n: kvbuf.at[pl.ds(dst * 512 + lo, n), :], dev(dz=-1))
+        for h in range(2):
+            if s < 4 or h == 0:
+                KP[s, h] = ring(0 if s == 1 else 2 * s - 3, 2 * s - 1, h * 128, dev(dz=1))
+            if s < 4 or h == 1:
+                KM[s, h] = ring(0 if s == 1 else 2 * s - 2, 2 * s if s < 4 else 7, h * 128, dev(dz=-1))
     for j in range(8):
         KD[j] = pool.copy(
             lambda j=j: kvbuf.at[pl.ds(j * 512, 256), :],
@@ -199,18 +213,22 @@
     WX = {"u": exchange(up_hbm, upbuf), "d": exchange(dn_hbm, dnbuf)}
     order = [0, -1, 1, -2, 2, -3, 3, 4]
 
+    xr = [0, -1, 1, 2]
+
     class Gather:
         def __init__(self, buf):
             a, b = (0, AW), (AW, W_COLS - AW)
             up, down, right, left = dev(dz=1), dev(dz=-1), dev(dx=1), dev(dx=-1)
             self.AP, self.AM, self.BP, self.BM = {}, {}, {}, {}
             for s in range(1, 5):
-                n, m = (64, 256) if s < 4 else (32, 128)
-                h, g = (0, 0) if s < 4 else (32, 128)
+                n, h = (64, 0) if s < 4 else (32, 32)
                 self.AP[s] = same(buf, (block(zat(1 - s), x), n), a, (block(zat(-s), x), n), up)
                 self.AM[s] = same(buf, (block(zat(s - 1), x) + h, n), a, (block(zat(s), x) + h, n), down)
-                self.BP[s] = same(buf, (block(zat(1 - s), 0), m), b, (block(zat(-s), 0), m), up)
-                self.BM[s] = same(buf, (block(zat(s - 1), 0) + g, m), b, (block(zat(s), 0) + g, m), down)
+                for i, r in enumerate(xr):
+                    if s < 4 or i < 2:
+                        self.BP[s, i] = same(buf, (block(zat(1 - s), xat(r)), 64), b, (block(zat(-s), xat(r)), 64), up)
+                    if s < 4 or i >= 2:
+                        self.BM[s, i] = same(buf, (block(zat(s - 1), xat(r)), 64), b, (block(zat(s), xat(r)), 64), down)
             self.ax = {d: self.spread(buf, zat(d), a, right, left) for d in order}
             self.bx = self.spread(buf, z, b, right, left)
 
@@ -223,24 +241,27 @@
             )
 
         def begin(self):
-            for t in (self.bx[0], self.bx[1], self.AP[1], self.AM[1], self.ax[0][0], self.ax[0][1]):
+            for t in (self.bx[0], self.bx[1], self.AP[1], self.AM[1], self.BP[1, 0], self.BM[1, 0], self.ax[0][0], self.ax[0][1]):
                 t.start()
 
-        def pass_on(self, sp4):
-            sp4[0].wait()
-            sp4[2].start()
-            sp4[1].wait()
-            sp4[3].start()
+        def pass_on(self, four):
+            four[0].wait()
+            four[2].start()
+            four[1].wait()
+            four[3].start()
 
         def first_x(self):
             self.pass_on(self.bx)
+            for i in (1, 2):
+                self.BP[1, i].start()
+                self.BM[1, i].start()
             self.pass_on(self.ax[0])
 
         def row(self):
             self.bx[2].wait()
             self.bx[3].wait()
-            self.BP[1].start()
-            self.BM[1].start()
+            self.BP[1, 3].start()
+            self.BM[1, 3].start()
 
         def a_step(self, s):
             self.AP[s].wait()
@@ -253,13 +274,12 @@
                 self.ax[d][0].start()
                 self.ax[d][1].start()
 
-        def b_step(self, s):
-            self.BP[s].wait()
-            if s < 4:
-                self.BP[s + 1].start()
-            self.BM[s].wait()
-            if s < 4:
-                self.BM[s + 1].start()
+        def b_step(self, s, i):
+            for chain in (self.BP, self.BM):
+                if (s, i) in chain:
+                    chain[s, i].wait()
+                    if (s + 1, i) in chain:
+                        chain[s + 1, i].start()
 
         def x_step(self, s):
             for d in (-s, s) if s < 4 else (4,):
@@ -269,11 +289,12 @@
             self.ax[d][2].wait()
             self.ax[d][3].wait()
 
-        def events(self):
-            steps = [self.begin, self.first_x, self.row]
-            for s in range(1, 4):
-                steps += [functools.partial(self.a_step, s), functools.partial(self.b_step, s), functools.partial(self.x_step, s)]
-            return steps + [functools.partial(self.a_step, 4), functools.partial(self.b_step, 4), functools.partial(self.x_step, 4)]
+        def groups(self):
+            out = [[self.begin], [self.first_x, self.row]]
+            for s in range(1, 5):
+                b = [functools.partial(self.b_step, s, i) for i in range(4)]
+                out.append([functools.partial(self.a_step, s), b[0], b[1], functools.partial(self.x_step, s), b[2], b[3]])
+            return out
 
     U, D = Gather(upbuf), Gather(dnbuf)
     DD = [pool.copy(lambda j=j: psend.at[j], lambda j=j: precv.at[j], lambda j=j: precv.at[j], flip) for j in range(8)]
@@ -282,50 +303,75 @@
         for j in range(8)
     ]
 
-    u, d = U.events(), D.events()
-    queue = u[0:6] + [d[0]] + u[6:9] + d[1:3] + u[9:12] + d[3:6] + u[12:15] + d[6:15]
+    ug, dg = U.groups(), D.groups()
+    u, d = sum(ug, []), sum(dg, [])
+    names = {id(e): t + str(i) + "_" + str(k) for t, gs in (("u", ug), ("d", dg)) for i, g in enumerate(gs) for k, e in enumerate(g)}
+
+    def run(e):
+        with jax.named_scope(names.get(id(e), "step")):
+            e()
+
+    def first(g):
+        return g[:3]
+
+    def second(g):
+        return g[4:]
+
+    def across(g):
+        return g[3:4]
+
+    queue = ug[0] + ug[1] + dg[0] + first(ug[2]) + second(ug[2]) + dg[1] + across(ug[2])
+    for s in (2, 3, 4):
+        queue += first(ug[s + 1]) + second(ug[s + 1])
+        if s > 2:
+            queue += across(dg[s - 1])
+        queue += first(dg[s]) + second(dg[s]) + across(ug[s + 1])
+    queue += first(dg[5]) + second(dg[5]) + across(dg[4]) + across(dg[5])
+    d = [e for e in queue if e in d]
     at = [0]
 
     def w(n):
         for e in queue[at[0] : at[0] + n]:
-            e()
+            run(e)
         at[0] += n
 
+    phase("p_barrier")
     pl.semaphore_wait(barrier, len(partners))
-    KP[1].start()
-    KM[1].start()
+    for h in range(2):
+        KP[1, h].start()
+        KM[1, h].start()
     KD[0].start()
     for i in (1, 3, 2):
         QS[i].start()
     WX["u"].start()
     WX["d"].start()
+    phase("p_wx")
     local[0].wait()
     WX["u"].wait()
     w(1)
     local[1].wait()
     WX["d"].wait()
-    KP[1].wait()
-    KP[2].start()
-    KD[1].start()
-    KM[1].wait()
-    KM[2].start()
-    KD[2].start()
-    for i in range(3):
-        KD[i].wait()
-    w(1)
-    for i in (1, 2, 3):
-        QS[i].wait()
-
+    phase("p_kv1")
     def kv_step(s):
-        KP[s].wait()
-        KM[s].wait()
+        for h in range(2):
+            for chain in (KP, KM):
+                if (s, h) in chain:
+                    chain[s, h].wait()
+                    if (s + 1, h) in chain:
+                        chain[s + 1, h].start()
         if s < 4:
-            KP[s + 1].start()
-            KM[s + 1].start()
             KD[2 * s - 1].start()
             KD[2 * s].start()
         else:
             KD[7].start()
+
+    kv_step(1)
+    for i in range(3):
+        KD[i].wait()
+    w(2)
+    phase("p_qwait")
+    for i in (1, 2, 3):
+        QS[i].wait()
 
     def scores(row, lo, hi):
         q = qbuf[pl.ds(row, 256), :]
@@ -352,7 +398,7 @@
             @pl.when(i == step)
             def _(fns=fns):
                 for f in fns:
-                    f()
+                    run(f)
 
     def pass1(i, _):
         row = pl.multiple_of((i + 2) % 8 * 256, 256)
@@ -369,8 +415,12 @@
         at[0] += n
         return got
 
-    ev1 = {1: [lambda: kv_step(2)], 2: grab(1), 4: [lambda: kv_step(3)] + grab(1), 6: grab(1), 7: grab(1) + [lambda: kv_step(4)]}
+    ev1 = {
+        0: [lambda: kv_step(2)], 1: grab(1), 2: grab(3), 3: [lambda: kv_step(3)], 4: grab(4), 5: grab(1), 6: [lambda: kv_step(4)], 7: grab(3),
+    }
+    phase("p_pass1")
     lax.fori_loop(0, 8, pass1, 0)
+    phase("p_kdwait")
     for i in range(3, 8):
         KD[i].wait()
 
@@ -399,14 +449,18 @@
         return 0
 
     ev2 = {
-        0: grab(1), 1: [lambda: send_o(1)], 2: grab(1), 3: [lambda: send_o(2)] + grab(1), 4: grab(1), 5: [lambda: send_o(3)], 6: grab(1), 7: grab(1),
+        0: grab(2), 1: [lambda: send_o(1)] + grab(3), 2: grab(3), 3: [lambda: send_o(2)] + grab(3), 4: grab(3), 5: [lambda: send_o(3)] + grab(3),
+        6: grab(3), 7: grab(3),
     }
+    phase("p_pass2")
     lax.fori_loop(0, 8, pass2, 0)
 
+    phase("p_owait")
     for i in (1, 2, 3):
         ST[i].wait()
     for i in (1, 2, 3):
         OS[i].wait()
+    phase("p_combine")
     eye = eye128()
     for g in range(4):
         rows = pl.ds(g * 128, 128)
@@ -422,38 +476,41 @@
             num += orecv[i, g * 128 : g * 128 + 128, :].astype(F32) * es[i]
             den += ls[i] * es[i]
         att_s[(g % 2) * 128 : (g % 2) * 128 + 128, (g // 2) * 128 : (g // 2) * 128 + 128] = (num / den).astype(BF16)
+    phase("p_att")
     for i in (1, 3, 2):
         AT[i].start()
     local[2].wait()
     local[3].wait()
-    w(1)
+    w(3)
     for i in (1, 2, 3):
         AT[i].wait()
+    phase("p_mixed")
     mixed = RESIDUAL_SCALE * res[...].astype(F32)
     for i in range(4):
         a = att_s[pl.ds(pl.multiple_of(y * 64, 64), 64), :] if i == 0 else attbuf[i]
         mixed += dot(a, ow[pl.ds(pl.multiple_of((y - i + NY) % NY * 256, 256), 256), :])
     xbuf[0:64, :] = layer_norm(mixed, fg_ref[...], fb_ref[...]).astype(BF16)
+    phase("p_yag")
     YP1.start()
     YM1.start()
     XD[0].start()
-    w(2)
+    w(3)
     YP1.wait()
     YP2.start()
     XD[1].start()
     YM1.wait()
     YM2.start()
     XD[3].start()
-    w(2)
+    w(3)
     YP2.wait()
     YM2.wait()
     XD[2].start()
-    w(2)
+    w(3)
     for i in range(4):
         XD[i].wait()
 
-    u_left = [f for f in u if f in queue[at[0] :]]
-    while any(f in queue[at[0] :] for f in u_left):
+    phase("p_uwait")
+    while any(f in u for f in queue[at[0] :]):
         w(1)
     for i in order:
         U.have(i)
@@ -464,6 +521,7 @@
         hid[:, cols] = (h * h).astype(BF16)
         return 0
 
+    phase("p_up")
     lax.fori_loop(0, 4, up_tile, 0)
 
     def combine(j, zs):
@@ -476,12 +534,12 @@
         for k in (1, 3, 2):
             RS[j][k - 1].start()
 
-    need = {0: d.index(d[5]) + 1, 1: 6, 2: 6, 3: 9, 4: 9, 5: 12, 6: 12, 7: 15}
+    phase("p_down")
+    need = {dz: max(i for i, e in enumerate(d) if any(e in g for g in dg[: abs(dz) + 2])) + 1 for dz in order}
     done_d = [len([f for f in d if f not in queue[at[0] :]])]
-    need[0] = 3
     for j, dz in enumerate(order):
-        while done_d[0] < need[j]:
-            d[done_d[0]]()
+        while done_d[0] < need[dz]:
+            run(d[done_d[0]])
             done_d[0] += 1
         D.have(dz)
         zs = zat(dz)
@@ -493,6 +551,7 @@
             combine(j - 1, zat(order[j - 1]))
     combine(7, zat(4))
 
+    phase("p_last")
     for j, dz in enumerate(order):
         cols = pl.ds(pl.multiple_of(zat(dz) * 256, 256), 256)
         for k in (1, 2, 3):
@@ -500,8 +559,10 @@
         fin[:, cols] = fin[:, cols] + (yrecv[j, 1].astype(F32) + yrecv[j, 2].astype(F32) + yrecv[j, 3].astype(F32))
     summed = RESIDUAL_SCALE * xbuf[0:64, :].astype(F32) + fin[...]
     out_ref[...] = layer_norm(summed, sg_ref[...], sb_ref[...]).astype(BF16)
+    phase("p_drain")
     for t in pool.all:
         t.drain()
+    phase(None)
 
 
 def per_device(
@@ -509,13 +570,10 @@
     second_gain, second_bias,
 ):
     cos, sin = rotary_tables()
-    sp = lax.axis_index("sp")
+    zero = np.zeros((256, 64), np.float32)
 
     def table(t):
-        t = jnp.asarray(t)
-        row = jnp.broadcast_to(lax.dynamic_slice_in_dim(t, sp * 4, 4, 0)[:, None, :], (4, GRID_W, 64))
-        col = jnp.broadcast_to(t[None, :GRID_W, :], (4, GRID_W, 64))
-        return jnp.concatenate([row, col], axis=-1).reshape(256, HEAD_DIM)
+        return jnp.asarray(np.concatenate([t, zero], 1)), jnp.asarray(np.concatenate([zero, t], 1)[:GRID_W])
 
     vmem, hbm = pl.BlockSpec(memory_space=pltpu.VMEM), pl.BlockSpec(memory_space=pl.ANY)
     scratch = [
@@ -550,13 +608,13 @@
     return pl.pallas_call(
         kernel,
         out_shape=jax.ShapeDtypeStruct((64, 2048), BF16),
-        in_specs=[vmem] * 11 + [hbm] * 4,
+        in_specs=[vmem] * 13 + [hbm] * 4,
         out_specs=vmem,
         scratch_shapes=scratch,
         compiler_params=pltpu.CompilerParams(collective_id=0, has_side_effects=True, vmem_limit_bytes=62 * 1024 * 1024),
         name="layer",
     )(
-        queries, keys, values, table(cos), table(sin), query_gain[None], key_gain[None], first_gain[None], first_bias[None],
+        queries, keys, values, *table(cos), *table(sin), query_gain[None], key_gain[None], first_gain[None], first_bias[None],
         second_gain[None], second_bias[None], residual, out_weight, up_weight, down_weight,
     )
 

time: 132 us -> 111 us (0.84)
  Pallas kernels: 126 us -> 109 us
  local copies, waits for them, and re-layouts: 3.94 us -> 1.67 us
  other arithmetic: 1.52 us -> 0 us
    pallas_call x1, Pallas kernels: 126 us -> 109 us  [per_device(): pl.pallas_call(kernel, out_shape=jax.ShapeDtypeStruct((64, 2048), BF16),...]
    broadcast_in_dim x4 -> x0, local copies, waits for them, and re-layouts: 1.56 us -> none  [the longest x2 1.54 us: table(): col = jnp.broadcast_to(t[None, :GRID_W, :], (4, GRID_W, 64))]
    concatenate x2 -> x0, other arithmetic: 1.52 us -> none  [table(): return jnp.concatenate([row, col], axis=-1).reshape(256, HEAD_DIM)]
where the time goes in v2:
time: 111 us
  Pallas kernels  109 us (98%)
  local copies, waits for them, and re-layouts  1.67 us (2%)
    pallas_call x1, Pallas kernels, per_device(): pl.pallas_call(kernel, out_shape=jax.ShapeDtypeStruct((64, 2048), BF16),...  109 us

profile of v2, /device:TPU:1, one launch (start us, length us, event | category | flops | bytes accessed | tf_op | source)
XLA Modules:
  0.0 110.6 jit_solution(18037604236838168645)
XLA Ops:
  0.0 109.0 %layer.1 = bf16[64,2048]{1,0:T(8,128)(2,1)} custom-call(bf16[256,256]{1,0:T(8,128)(2,1)} %q_ref.1, bf16[256,128]{1,0:T(8,128)(2,1)} %k_ref.1, bf16[256,128]{1,0:T(8,128)(2,1)} %v_ref.1, f32[256,128]{1,0:T(8,128)} %constant.8.clone.cosr_ref, f32[64,128]{1,0:T(8,128)} %constant.9.clone.cosc_ref, f32[256,128]{1,0:T(8,128)} %constant.10.clone.sinr_ref, ...), custom_call_target="tpu_custom_call" | custom-call | tf_op jit(solution)/shard_map/layer/pallas_call | solution.py:608
  109.0 1.7 %copy.19 = bf16[64,2048]{1,0:T(8,128)(2,1)} copy(bf16[64,2048]{1,0:T(8,128)(2,1)} %layer.1) | data formatting | bytes 524288

commit v3 on v2

--- a/solution.py
+++ b/solution.py
@@ -19,7 +19,7 @@
 SCALE2 = float(np.log2(np.e) * HEAD_DIM**-0.5)
 AW = 640
 W_COLS = 1024
-PASS1 = 3 * 512
+PASS1, PASS2 = 3 * 512, 5 * 512
 KEYS = 4096
 F32, BF16 = jnp.float32, jnp.bfloat16
 
@@ -83,7 +83,7 @@
         return c
 
 
-N_SEMS = 240
+N_SEMS = 264
 
 
 def layer_norm(summed, gain, bias):
@@ -100,10 +100,6 @@
     return (x * cos + swapped * sin).astype(BF16)
 
 
-def eye128():
-    return lax.broadcasted_iota(jnp.int32, (128, 128), 0) == lax.broadcasted_iota(jnp.int32, (128, 128), 1)
-
-
 def dot(a, b, dims=((1,), (0,))):
     return lax.dot_general(a, b, (dims, ((), ())), preferred_element_type=F32)
 
@@ -112,7 +108,7 @@
     q_ref, k_ref, v_ref, cosr_ref, cosc_ref, sinr_ref, sinc_ref, qg_ref, kg_ref, fg_ref, fb_ref, sg_ref, sb_ref,
     res_hbm, ow_hbm, up_hbm, dn_hbm,
     out_ref,
-    kvbuf, qbuf, o_acc, m_acc, l_acc, s_scr, osend, orecv, stsend, strecv, att_s, attbuf, ow, res, xbuf,
+    kbuf, vtbuf, qbuf, o_acc, m_acc, l_acc, s_even, s_odd, osend, orecv, stsend, strecv, att_s, attbuf, ow, res, xbuf,
     upbuf, dnbuf, hid, psend, precv, pown, ysend, yrecv, fin,
     ssem, rsem, lsem,
 ):
@@ -160,8 +156,8 @@
         return jnp.concatenate(parts, axis=0)
 
     cos, sin = angles(cosr_ref, cosc_ref), angles(sinr_ref, sinc_ref)
-    kvbuf[0:256, 0:128] = norm_rotate(k_ref[...], kg_ref[...], cos, sin)
-    kvbuf[0:256, 128:256] = v_ref[...]
+    kbuf[0:256, :] = norm_rotate(k_ref[...], kg_ref[...], cos, sin)
+    vtbuf[:, 0:256] = jnp.transpose(v_ref[...].astype(F32)).astype(BF16)
     qbuf[0:256, :] = norm_rotate(q_ref[:, 0:128], qg_ref[...], cos, sin)
     qbuf[256:512, :] = norm_rotate(q_ref[:, 128:256], qg_ref[...], cos, sin)
 
@@ -172,27 +168,41 @@
     flip = dev(flip=True)
     KP, KM, KD = {}, {}, {}
 
-    def ring(src, dst, lo, device):
-        view = lambda slot: kvbuf.at[pl.ds(slot * 512 + lo, 128), :]
-        return pool.copy(lambda: view(src), lambda: view(dst), lambda: view(dst), device)
+    def place(at_key, h):
+        return kbuf.at[pl.ds(at_key, 256), :] if h == 0 else vtbuf.at[:, pl.ds(at_key, 256)]
+
+    def ring(src, dst, h, device):
+        return pool.copy(lambda: place(src * 512, h), lambda: place(dst * 512, h), lambda: place(dst * 512, h), device)
 
     for s in range(1, 5):
         for h in range(2):
             if s < 4 or h == 0:
-                KP[s, h] = ring(0 if s == 1 else 2 * s - 3, 2 * s - 1, h * 128, dev(dz=1))
+                KP[s, h] = ring(0 if s == 1 else 2 * s - 3, 2 * s - 1, h, dev(dz=1))
             if s < 4 or h == 1:
-                KM[s, h] = ring(0 if s == 1 else 2 * s - 2, 2 * s if s < 4 else 7, h * 128, dev(dz=-1))
+                KM[s, h] = ring(0 if s == 1 else 2 * s - 2, 2 * s if s < 4 else 7, h, dev(dz=-1))
+    class Both(list):
+        def start(self):
+            for t in self:
+                t.start()
+
+        def wait(self):
+            for t in self:
+                t.wait()
+
+    def to_other(j, h):
+        there = lambda: place(j * 512 + 256, h)
+        return pool.copy(lambda: place(j * 512, h), there, there, flip)
+
     for j in range(8):
-        KD[j] = pool.copy(
-            lambda j=j: kvbuf.at[pl.ds(j * 512, 256), :],
-            lambda j=j: kvbuf.at[pl.ds(j * 512 + 256, 256), :],
-            lambda j=j: kvbuf.at[pl.ds(j * 512 + 256, 256), :], flip)
+        KD[j] = Both(to_other(j, h) for h in range(2))
     QS, OS, ST, AT = {}, {}, {}, {}
     for d in range(1, 4):
         QS[d] = pool.copy(
             lambda: qbuf.at[pl.ds(0, 512), :], lambda d=d: qbuf.at[pl.ds(d * 512, 512), :],
             lambda d=d: qbuf.at[pl.ds(d * 512, 512), :], dev(dx=d))
-        OS[d] = pool.copy(lambda d=d: osend.at[d], lambda d=d: orecv.at[d], lambda d=d: orecv.at[d], dev(dx=-d))
+        for h in range(2):
+            OS[d, h] = pool.copy(
+                lambda d=d, h=h: osend.at[d, h], lambda d=d, h=h: orecv.at[d, h], lambda d=d, h=h: orecv.at[d, h], dev(dx=-d))
         ST[d] = pool.copy(lambda d=d: stsend.at[d], lambda d=d: strecv.at[d], lambda d=d: strecv.at[d], dev(dx=-d))
         AT[d] = pool.copy(
             lambda d=d: att_s.at[pl.ds(pl.multiple_of((y + d) % NY * 64, 64), 64), :],
@@ -200,11 +210,11 @@
     def rows_of(ref, lo, n):
         return lambda: ref.at[pl.ds(lo, n), :]
 
-    YP1 = pool.copy(rows_of(xbuf, 0, 64), rows_of(xbuf, 64, 64), rows_of(xbuf, 64, 64), dev(dy=1))
-    YM1 = pool.copy(rows_of(xbuf, 0, 64), rows_of(xbuf, 192, 64), rows_of(xbuf, 192, 64), dev(dy=-1))
-    YP2 = pool.copy(rows_of(xbuf, 64, 32), rows_of(xbuf, 128, 32), rows_of(xbuf, 128, 32), dev(dy=1))
-    YM2 = pool.copy(rows_of(xbuf, 224, 32), rows_of(xbuf, 160, 32), rows_of(xbuf, 160, 32), dev(dy=-1))
-    XD = [pool.copy(rows_of(xbuf, j * 64, 64), rows_of(xbuf, 256 + j * 64, 64), rows_of(xbuf, 256 + j * 64, 64), flip) for j in range(4)]
+    YP = [pool.copy(rows_of(xbuf, h, 32), rows_of(xbuf, 128 + h, 32), rows_of(xbuf, 128 + h, 32), dev(dy=1)) for h in (0, 32)]
+    YM = [pool.copy(rows_of(xbuf, h, 32), rows_of(xbuf, 384 + h, 32), rows_of(xbuf, 384 + h, 32), dev(dy=-1)) for h in (32, 0)]
+    YP2 = pool.copy(rows_of(xbuf, 128, 32), rows_of(xbuf, 256, 32), rows_of(xbuf, 256, 32), dev(dy=1))
+    YM2 = pool.copy(rows_of(xbuf, 416, 32), rows_of(xbuf, 288, 32), rows_of(xbuf, 288, 32), dev(dy=-1))
+    XD = [pool.copy(rows_of(xbuf, j * 128, 64), rows_of(xbuf, j * 128 + 64, 64), rows_of(xbuf, j * 128 + 64, 64), flip) for j in range(4)]
 
     def exchange(hbm, buf):
         return pool.copy(
@@ -240,28 +250,11 @@
                 same(buf, (block(zs, xat(1)) + 32, 32), cols, (block(zs, xat(2)) + 32, 32), left),
             )
 
-        def begin(self):
-            for t in (self.bx[0], self.bx[1], self.AP[1], self.AM[1], self.BP[1, 0], self.BM[1, 0], self.ax[0][0], self.ax[0][1]):
-                t.start()
-
         def pass_on(self, four):
             four[0].wait()
             four[2].start()
             four[1].wait()
             four[3].start()
-
-        def first_x(self):
-            self.pass_on(self.bx)
-            for i in (1, 2):
-                self.BP[1, i].start()
-                self.BM[1, i].start()
-            self.pass_on(self.ax[0])
-
-        def row(self):
-            self.bx[2].wait()
-            self.bx[3].wait()
-            self.BP[1, 3].start()
-            self.BM[1, 3].start()
 
         def a_step(self, s):
             self.AP[s].wait()
@@ -289,8 +282,27 @@
             self.ax[d][2].wait()
             self.ax[d][3].wait()
 
+        def early(self):
+            for t in (self.bx[0], self.bx[1], self.ax[0][0], self.ax[0][1]):
+                t.start()
+
+        def early_on(self):
+            self.pass_on(self.bx)
+
+        def late(self):
+            for t in (self.AP[1], self.AM[1], self.BP[1, 0], self.BM[1, 0]):
+                t.start()
+            self.bx[2].wait()
+            self.bx[3].wait()
+            for i in (1, 2, 3):
+                self.BP[1, i].start()
+                self.BM[1, i].start()
+
+        def own_on(self):
+            self.pass_on(self.ax[0])
+
         def groups(self):
-            out = [[self.begin], [self.first_x, self.row]]
+            out = [[self.early], [self.early_on, self.late, self.own_on]]
             for s in range(1, 5):
                 b = [functools.partial(self.b_step, s, i) for i in range(4)]
                 out.append([functools.partial(self.a_step, s), b[0], b[1], functools.partial(self.x_step, s), b[2], b[3]])
@@ -320,13 +332,13 @@
     def across(g):
         return g[3:4]
 
-    queue = ug[0] + ug[1] + dg[0] + first(ug[2]) + second(ug[2]) + dg[1] + across(ug[2])
-    for s in (2, 3, 4):
-        queue += first(ug[s + 1]) + second(ug[s + 1])
-        if s > 2:
-            queue += across(dg[s - 1])
-        queue += first(dg[s]) + second(dg[s]) + across(ug[s + 1])
-    queue += first(dg[5]) + second(dg[5]) + across(dg[4]) + across(dg[5])
+    def step(g):
+        return first(g) + second(g)
+
+    queue = ug[0] + dg[0] + ug[1] + dg[1][:1] + dg[1][2:] + step(ug[2])
+    queue += across(ug[2]) + dg[1][1:2] + step(ug[3]) + across(ug[3]) + step(ug[4]) + step(dg[2])
+    queue += across(ug[4]) + step(ug[5]) + across(dg[2]) + across(ug[5]) + step(dg[3])
+    queue += across(dg[3]) + step(dg[4]) + across(dg[4]) + step(dg[5]) + across(dg[5])
     d = [e for e in queue if e in d]
     at = [0]
 
@@ -351,6 +363,7 @@
     w(1)
     local[1].wait()
     WX["d"].wait()
+    w(1)
     phase("p_kv1")
     def kv_step(s):
         for h in range(2):
@@ -368,30 +381,60 @@
     kv_step(1)
     for i in range(3):
         KD[i].wait()
-    w(2)
     phase("p_qwait")
-    for i in (1, 2, 3):
-        QS[i].wait()
-
-    def scores(row, lo, hi):
-        q = qbuf[pl.ds(row, 256), :]
-        best = None
+
+    def tile_scores(t, at_key, dst, lo, best):
+        q = qbuf[pl.ds(pl.multiple_of(t * 256, 256), 256), :]
+        part = dot(kbuf[pl.ds(at_key, 512), :], q, ((1,), (1,)))
+        dst[pl.ds(at_key - lo, 512), :] = part
+        top = jnp.max(part.reshape(64, 8, 256), axis=0)
+        return top if best is None else jnp.maximum(best, top)
+
+    def stage(t_next, t, src, dst, m, lo, hi):
+        best, total, out = None, None, None
         for at_key in range(lo, hi, 512):
-            part = dot(q, kvbuf[pl.ds(at_key, 512), 0:128], ((1,), (1,)))
-            s_scr[:, pl.ds(at_key - lo, 512)] = part
-            for g in range(0, 512, 128):
-                best = part[:, g : g + 128] if best is None else jnp.maximum(best, part[:, g : g + 128])
-        return jnp.max(best, axis=1, keepdims=True)
-
-    def weigh(m, lo, hi):
-        total, out = None, None
+            best = tile_scores(t_next, at_key, dst, lo, best)
+            p = jnp.exp2((src[pl.ds(at_key - lo, 512), :] - m) * SCALE2)
+            part = jnp.sum(p.reshape(64, 8, 256), axis=0)
+            o = dot(vtbuf[:, pl.ds(at_key, 512)], p.astype(BF16))
+            total, out = (part, o) if total is None else (total + part, out + o)
+        l = jnp.sum(total, axis=0, keepdims=True)
+        m_next = jnp.max(best, axis=0, keepdims=True)
+        if lo > 0:
+            m_old = m_acc[t, 0:1, :]
+            alpha = jnp.exp2((m_old - m) * SCALE2)
+            out = o_acc[t] * alpha + out
+            l = l_acc[t, 0:1, :] * alpha + l
+            m_next = jnp.maximum(m_next, m_acc[t_next, 0:1, :])
+        if hi == KEYS:
+            upper = lax.broadcasted_iota(jnp.int32, (8, 256), 0) < 4
+            stsend[t // 2, t % 2] = jnp.where(upper, jnp.broadcast_to(m, (8, 256)), jnp.broadcast_to(l, (8, 256)))
+            osend[t // 2, t % 2] = out.astype(BF16)
+        o_acc[t] = out
+        m_acc[t] = jnp.broadcast_to(m, (8, 256))
+        l_acc[t] = jnp.broadcast_to(l, (8, 256))
+        return m_next
+
+    def all_tiles(lo, hi, table):
+        def slot_of(i):
+            return (2 + i * (i + 1) // 2) % 4 if hi == KEYS else i % 4
+
+        best, t = None, 2 * slot_of(0)
         for at_key in range(lo, hi, 512):
-            p = jnp.exp2((s_scr[:, pl.ds(at_key - lo, 512)] - m) * SCALE2)
-            for g in range(0, 512, 128):
-                total = p[:, g : g + 128] if total is None else total + p[:, g : g + 128]
-            o = dot(p.astype(BF16), kvbuf[pl.ds(at_key, 512), 128:256])
-            out = o if out is None else out + o
-        return jnp.sum(total, axis=1, keepdims=True), out
+            best = tile_scores(t, at_key, s_even, lo, best)
+        m = jnp.max(best, axis=0, keepdims=True)
+        if lo > 0:
+            m = jnp.maximum(m, m_acc[t, 0:1, :])
+
+        def two(i, m):
+            t = 2 * slot_of(i)
+            m = stage(t + 1, t, s_even, s_odd, m, lo, hi)
+            events_at(i, {k // 2: f for k, f in table.items() if k % 2 == 0})
+            m = stage(2 * slot_of(i + 1), t + 1, s_odd, s_even, m, lo, hi)
+            events_at(i, {k // 2: f for k, f in table.items() if k % 2 == 1})
+            return m
+
+        lax.fori_loop(0, 4, two, m)
 
     def events_at(i, table):
         for step, fns in table.items():
@@ -400,88 +443,71 @@
                 for f in fns:
                     run(f)
 
-    def pass1(i, _):
-        row = pl.multiple_of((i + 2) % 8 * 256, 256)
-        m = scores(row, 0, PASS1)
-        l, o = weigh(m, 0, PASS1)
-        o_acc[pl.ds(row, 256), :] = o
-        m_acc[pl.ds(row, 256), :] = jnp.broadcast_to(m, (256, 128))
-        l_acc[pl.ds(row, 256), :] = jnp.broadcast_to(l, (256, 128))
-        events_at(i, ev1)
-        return 0
-
     def grab(n):
         got = queue[at[0] : at[0] + n]
         at[0] += n
         return got
 
+    def queries_from(*who):
+        return [lambda: [QS[i].wait() for i in who]]
+
     ev1 = {
-        0: [lambda: kv_step(2)], 1: grab(1), 2: grab(3), 3: [lambda: kv_step(3)], 4: grab(4), 5: grab(1), 6: [lambda: kv_step(4)], 7: grab(3),
+        0: queries_from(1, 3) + grab(1), 1: [lambda: kv_step(2)], 2: queries_from(2) + grab(1), 4: grab(1), 5: grab(1), 6: grab(1),
     }
+    ev2 = {0: [lambda: kv_step(3)], 7: [lambda: kv_step(4)]}
     phase("p_pass1")
-    lax.fori_loop(0, 8, pass1, 0)
+    all_tiles(0, PASS1, ev1)
+    phase("p_pass1b")
+    for i in (3, 4):
+        KD[i].wait()
+    all_tiles(PASS1, PASS2, ev2)
     phase("p_kdwait")
-    for i in range(3, 8):
+    w(5)
+    for i in (5, 6, 7):
         KD[i].wait()
 
-    def send_o(d):
-        eye = eye128()
-        for g in range(4):
-            rows = pl.ds(d * 512 + g * 128, 128)
-            stsend[d, g : g + 1, :] = jnp.sum(jnp.where(eye, m_acc[rows, :], 0.0), axis=0, keepdims=True)
-            stsend[d, g + 4 : g + 5, :] = jnp.sum(jnp.where(eye, l_acc[rows, :], 0.0), axis=0, keepdims=True)
-        OS[d].start()
-        ST[d].start()
-
-    def pass2(i, _):
-        row = pl.multiple_of((i + 2) % 8 * 256, 256)
-        m_old = m_acc[pl.ds(row, 256), 0:1]
-        m = jnp.maximum(scores(row, PASS1, KEYS), m_old)
-        alpha = jnp.exp2((m_old - m) * SCALE2)
-        l, o = weigh(m, PASS1, KEYS)
-        o = o_acc[pl.ds(row, 256), :] * alpha + o
-        l = l_acc[pl.ds(row, 256), 0:1] * alpha + l
-        o_acc[pl.ds(row, 256), :] = o
-        m_acc[pl.ds(row, 256), :] = jnp.broadcast_to(m, (256, 128))
-        l_acc[pl.ds(row, 256), :] = jnp.broadcast_to(l, (256, 128))
-        osend[row // 512, pl.ds(pl.multiple_of(row % 512, 256), 256), :] = o.astype(BF16)
-        events_at(i, ev2)
-        return 0
-
-    ev2 = {
-        0: grab(2), 1: [lambda: send_o(1)] + grab(3), 2: grab(3), 3: [lambda: send_o(2)] + grab(3), 4: grab(3), 5: [lambda: send_o(3)] + grab(3),
-        6: grab(3), 7: grab(3),
-    }
+    def send_o(d, h):
+        def go():
+            OS[d, h].start()
+            if h == 1:
+                ST[d].start()
+
+        return [go]
+
+    ev3 = {2 * i + h: send_o(d, h) for i, d in enumerate((2, 3, 1)) for h in range(2)}
+    for k, n in ((1, 1), (3, 1), (5, 3)):
+        ev3[k] = ev3[k] + grab(n)
     phase("p_pass2")
-    lax.fori_loop(0, 8, pass2, 0)
+    all_tiles(PASS2, KEYS, ev3)
 
     phase("p_owait")
+    w(6)
     for i in (1, 2, 3):
         ST[i].wait()
     for i in (1, 2, 3):
-        OS[i].wait()
+        OS[i, 0].wait()
+        OS[i, 1].wait()
     phase("p_combine")
-    eye = eye128()
-    for g in range(4):
-        rows = pl.ds(g * 128, 128)
-        ms, ls = [m_acc[rows, 0:1]], [l_acc[rows, 0:1]]
+    for h in range(2):
+        ms, ls = [m_acc[h, 0:1, :]], [l_acc[h, 0:1, :]]
         for i in (1, 2, 3):
-            ms.append(jnp.sum(jnp.where(eye, strecv[i, g : g + 1, :], 0.0), axis=1, keepdims=True))
-            ls.append(jnp.sum(jnp.where(eye, strecv[i, g + 4 : g + 5, :], 0.0), axis=1, keepdims=True))
+            ms.append(strecv[i, h, 0:1, :])
+            ls.append(strecv[i, h, 4:5, :])
         top = jnp.maximum(jnp.maximum(ms[0], ms[1]), jnp.maximum(ms[2], ms[3]))
         es = [jnp.exp2((m - top) * SCALE2) for m in ms]
-        num = o_acc[rows, :] * es[0]
+        num = o_acc[h] * es[0]
         den = ls[0] * es[0]
         for i in (1, 2, 3):
-            num += orecv[i, g * 128 : g * 128 + 128, :].astype(F32) * es[i]
+            num += orecv[i, h].astype(F32) * es[i]
             den += ls[i] * es[i]
-        att_s[(g % 2) * 128 : (g % 2) * 128 + 128, (g // 2) * 128 : (g // 2) * 128 + 128] = (num / den).astype(BF16)
+        att_s[:, h * 128 : h * 128 + 128] = jnp.transpose(num / den).astype(BF16)
     phase("p_att")
     for i in (1, 3, 2):
         AT[i].start()
     local[2].wait()
     local[3].wait()
-    w(3)
+    w(7)
+    phase("q_atwait")
     for i in (1, 2, 3):
         AT[i].wait()
     phase("p_mixed")
@@ -491,41 +517,56 @@
         mixed += dot(a, ow[pl.ds(pl.multiple_of((y - i + NY) % NY * 256, 256), 256), :])
     xbuf[0:64, :] = layer_norm(mixed, fg_ref[...], fb_ref[...]).astype(BF16)
     phase("p_yag")
-    YP1.start()
-    YM1.start()
-    XD[0].start()
+    for t in (YP[0], YM[0], YP[1], YM[1], XD[0]):
+        t.start()
+    w(7)
+    phase("q_yp1")
+    YP[0].wait()
+    YP2.start()
+    YM[0].wait()
+    YM2.start()
+    YP[1].wait()
+    XD[1].start()
+    YM[1].wait()
+    XD[3].start()
+    w(6)
+    assert not any(e in u for e in queue[at[0] :])
+    phase("q_uhave")
+    for i in order:
+        U.have(i)
+
+    def up_rows(lo):
+        def tile(i, _):
+            cols = pl.ds(pl.multiple_of(i * 256, 256), 256)
+            h = jnp.maximum(dot(xbuf[pl.ds(lo, 128), :], upbuf[:, cols]), 0.0)
+            hid[pl.ds(lo, 128), cols] = (h * h).astype(BF16)
+            return 0
+
+        lax.fori_loop(0, 4, tile, 0)
+
+    phase("q_up0")
+    XD[0].wait()
+    up_rows(0)
+    w(1)
+    XD[1].wait()
+    up_rows(128)
     w(3)
-    YP1.wait()
-    YP2.start()
-    XD[1].start()
-    YM1.wait()
-    YM2.start()
-    XD[3].start()
-    w(3)
+    XD[3].wait()
+    up_rows(384)
+    w(2)
+    phase("q_yp2")
     YP2.wait()
     YM2.wait()
     XD[2].start()
-    w(3)
-    for i in range(4):
-        XD[i].wait()
-
-    phase("p_uwait")
-    while any(f in u for f in queue[at[0] :]):
-        w(1)
-    for i in order:
-        U.have(i)
-
-    def up_tile(i, _):
-        cols = pl.ds(pl.multiple_of(i * 256, 256), 256)
-        h = jnp.maximum(dot(xbuf[...], upbuf[:, cols]), 0.0)
-        hid[:, cols] = (h * h).astype(BF16)
-        return 0
-
-    phase("p_up")
-    lax.fori_loop(0, 4, up_tile, 0)
+    phase("q_xd")
+    XD[2].wait()
+    phase("q_up2")
+    up_rows(256)
 
     def combine(j, zs):
+        phase("q_ddwait")
         DD[j].wait()
+        phase("q_comb")
         cols = pl.ds(pl.multiple_of(zs * 256, 256), 256)
         both = pown[j % 2] + precv[j].astype(F32)
         fin[:, cols] = both[0:64]
@@ -536,16 +577,20 @@
 
     phase("p_down")
     need = {dz: max(i for i, e in enumerate(d) if any(e in g for g in dg[: abs(dz) + 2])) + 1 for dz in order}
+    ahead = {0: len(d) - 7, 1: len(d) - 3, 2: len(d) - 1, 3: len(d) - 1}
     done_d = [len([f for f in d if f not in queue[at[0] :]])]
     for j, dz in enumerate(order):
-        while done_d[0] < need[dz]:
+        while done_d[0] < max(need[dz], ahead.get(j, len(d))):
             run(d[done_d[0]])
             done_d[0] += 1
+        phase("q_have")
         D.have(dz)
+        phase("q_dot")
         zs = zat(dz)
         part = dot(hid[...], dnbuf[pl.ds(pl.multiple_of(zs * 256, 256), 256), :], ((1,), (1,)))
-        pown[j % 2] = part[0:256]
-        psend[j] = part[256:512].astype(BF16)
+        for i in range(4):
+            pown[j % 2, i * 64 : i * 64 + 64, :] = part[i * 128 : i * 128 + 64]
+            psend[j, i * 64 : i * 64 + 64, :] = part[i * 128 + 64 : i * 128 + 128].astype(BF16)
         DD[j].start()
         if j > 0:
             combine(j - 1, zat(order[j - 1]))
@@ -554,8 +599,10 @@
     phase("p_last")
     for j, dz in enumerate(order):
         cols = pl.ds(pl.multiple_of(zat(dz) * 256, 256), 256)
+        phase("q_rswait")
         for k in (1, 2, 3):
             RS[j][k - 1].wait()
+        phase("q_fin")
         fin[:, cols] = fin[:, cols] + (yrecv[j, 1].astype(F32) + yrecv[j, 2].astype(F32) + yrecv[j, 3].astype(F32))
     summed = RESIDUAL_SCALE * xbuf[0:64, :].astype(F32) + fin[...]
     out_ref[...] = layer_norm(summed, sg_ref[...], sb_ref[...]).astype(BF16)
@@ -577,16 +624,18 @@
 
     vmem, hbm = pl.BlockSpec(memory_space=pltpu.VMEM), pl.BlockSpec(memory_space=pl.ANY)
     scratch = [
-        pltpu.VMEM((KEYS, 256), BF16),
+        pltpu.VMEM((KEYS, 128), BF16),
+        pltpu.VMEM((128, KEYS), BF16),
         pltpu.VMEM((2048, 128), BF16),
-        pltpu.VMEM((2048, 128), F32),
-        pltpu.VMEM((2048, 128), F32),
-        pltpu.VMEM((2048, 128), F32),
-        pltpu.VMEM((256, KEYS - PASS1), F32),
-        pltpu.VMEM((4, 512, 128), BF16),
-        pltpu.VMEM((4, 512, 128), BF16),
-        pltpu.VMEM((4, 8, 128), F32),
-        pltpu.VMEM((4, 8, 128), F32),
+        pltpu.VMEM((8, 128, 256), F32),
+        pltpu.VMEM((8, 8, 256), F32),
+        pltpu.VMEM((8, 8, 256), F32),
+        pltpu.VMEM((1536, 256), F32),
+        pltpu.VMEM((1536, 256), F32),
+        pltpu.VMEM((4, 2, 128, 256), BF16),
+        pltpu.VMEM((4, 2, 128, 256), BF16),
+        pltpu.VMEM((4, 2, 8, 256), F32),
+        pltpu.VMEM((4, 2, 8, 256), F32),
         pltpu.VMEM((256, 256), BF16),
         pltpu.VMEM((4, 64, 256), BF16),
         pltpu.VMEM((1024, 2048), BF16),

time: 111 us -> 99.4 us (0.90)
  Pallas kernels: 109 us -> 97.6 us
    pallas_call x1, Pallas kernels: 109 us -> 97.6 us  [per_device(): pl.pallas_call(kernel, out_shape=jax.ShapeDtypeStruct((64, 2048), BF16),...]
where the time goes in v3:
time: 99.4 us; the launch traced here: 99.3 us
  Pallas kernels  97.6 us (98%)
  local copies, waits for them, and re-layouts  1.67 us (2%)
    pallas_call x1, Pallas kernels, per_device(): pl.pallas_call(kernel, out_shape=jax.ShapeDtypeStruct((64, 2048), BF16),...  97.6 us

profile of v3, /device:TPU:1, one launch (start us, length us, event | category | flops | bytes accessed | tf_op | source)
XLA Modules:
  0.0 99.3 jit_solution(574166040783289519)
XLA Ops:
  0.0 97.6 %layer.1 = bf16[64,2048]{1,0:T(8,128)(2,1)} custom-call(bf16[256,256]{1,0:T(8,128)(2,1)} %q_ref.1, bf16[256,128]{1,0:T(8,128)(2,1)} %k_ref.1, bf16[256,128]{1,0:T(8,128)(2,1)} %v_ref.1, f32[256,128]{1,0:T(8,128)} %constant.8.clone.cosr_ref, f32[64,128]{1,0:T(8,128)} %constant.9.clone.cosc_ref, f32[256,128]{1,0:T(8,128)} %constant.10.clone.sinr_ref, ...), custom_call_target="tpu_custom_call" | custom-call | tf_op jit(solution)/shard_map/layer/pallas_call | solution.py:657
  97.6 1.7 %copy.19 = bf16[64,2048]{1,0:T(8,128)(2,1)} copy(bf16[64,2048]{1,0:T(8,128)(2,1)} %layer.1) | data formatting | bytes 524288

commit v4 on v3

--- a/solution.py
+++ b/solution.py
@@ -481,7 +481,7 @@
     all_tiles(PASS2, KEYS, ev3)
 
     phase("p_owait")
-    w(6)
+    w(2)
     for i in (1, 2, 3):
         ST[i].wait()
     for i in (1, 2, 3):
@@ -506,7 +506,7 @@
         AT[i].start()
     local[2].wait()
     local[3].wait()
-    w(7)
+    w(11)
     phase("q_atwait")
     for i in (1, 2, 3):
         AT[i].wait()
@@ -531,37 +531,33 @@
     XD[3].start()
     w(6)
     assert not any(e in u for e in queue[at[0] :])
+    YP2.wait()
+    YM2.wait()
+    XD[2].start()
     phase("q_uhave")
     for i in order:
         U.have(i)
 
-    def up_rows(lo):
+    def up_rows(lo, n):
         def tile(i, _):
             cols = pl.ds(pl.multiple_of(i * 256, 256), 256)
-            h = jnp.maximum(dot(xbuf[pl.ds(lo, 128), :], upbuf[:, cols]), 0.0)
-            hid[pl.ds(lo, 128), cols] = (h * h).astype(BF16)
+            h = jnp.maximum(dot(xbuf[pl.ds(lo, n), :], upbuf[:, cols]), 0.0)
+            hid[pl.ds(lo, n), cols] = (h * h).astype(BF16)
             return 0
 
         lax.fori_loop(0, 4, tile, 0)
 
     phase("q_up0")
     XD[0].wait()
-    up_rows(0)
-    w(1)
     XD[1].wait()
-    up_rows(128)
-    w(3)
+    up_rows(0, 256)
+    w(4)
+    phase("q_xd")
     XD[3].wait()
-    up_rows(384)
-    w(2)
-    phase("q_yp2")
-    YP2.wait()
-    YM2.wait()
-    XD[2].start()
-    phase("q_xd")
     XD[2].wait()
     phase("q_up2")
-    up_rows(256)
+    up_rows(256, 256)
+    w(2)
 
     def combine(j, zs):
         phase("q_ddwait")

time: 99.4 us -> 98.8 us (level)
  no operation moved by 1% of the time
where the time goes in v4:
time: 98.8 us; the launch traced here: 98.7 us
  Pallas kernels  97 us (98%)
  local copies, waits for them, and re-layouts  1.67 us (2%)
    pallas_call x1, Pallas kernels, per_device(): pl.pallas_call(kernel, out_shape=jax.ShapeDtypeStruct((64, 2048), BF16),...  97 us

profile of v4, /device:TPU:1, one launch (start us, length us, event | category | flops | bytes accessed | tf_op | source)
XLA Modules:
  0.0 98.7 jit_solution(6981336586206274125)
XLA Ops:
  0.0 97.0 %layer.1 = bf16[64,2048]{1,0:T(8,128)(2,1)} custom-call(bf16[256,256]{1,0:T(8,128)(2,1)} %q_ref.1, bf16[256,128]{1,0:T(8,128)(2,1)} %k_ref.1, bf16[256,128]{1,0:T(8,128)(2,1)} %v_ref.1, f32[256,128]{1,0:T(8,128)} %constant.8.clone.cosr_ref, f32[64,128]{1,0:T(8,128)} %constant.9.clone.cosc_ref, f32[256,128]{1,0:T(8,128)} %constant.10.clone.sinr_ref, ...), custom_call_target="tpu_custom_call" | custom-call | tf_op jit(solution)/shard_map/layer/pallas_call | solution.py:653
  97.0 1.7 %copy.19 = bf16[64,2048]{1,0:T(8,128)(2,1)} copy(bf16[64,2048]{1,0:T(8,128)(2,1)} %layer.1) | data formatting | bytes 524288

commit v5 on v4

--- a/solution.py
+++ b/solution.py
@@ -573,7 +573,7 @@
 
     phase("p_down")
     need = {dz: max(i for i, e in enumerate(d) if any(e in g for g in dg[: abs(dz) + 2])) + 1 for dz in order}
-    ahead = {0: len(d) - 7, 1: len(d) - 3, 2: len(d) - 1, 3: len(d) - 1}
+    ahead = {0: len(d) - 7, 1: len(d) - 7, 2: len(d) - 6, 3: len(d) - 3, 4: len(d) - 1}
     done_d = [len([f for f in d if f not in queue[at[0] :]])]
     for j, dz in enumerate(order):
         while done_d[0] < max(need[dz], ahead.get(j, len(d))):

time: 98.8 us -> 96.3 us (0.975)
  Pallas kernels: 97 us -> 94.5 us
    pallas_call x1, Pallas kernels: 97 us -> 94.5 us  [per_device(): pl.pallas_call(kernel, out_shape=jax.ShapeDtypeStruct((64, 2048), BF16),...]
where the time goes in v5:
time: 96.3 us; the launch traced here: 96.2 us
  Pallas kernels  94.5 us (98%)
  local copies, waits for them, and re-layouts  1.67 us (2%)
    pallas_call x1, Pallas kernels, per_device(): pl.pallas_call(kernel, out_shape=jax.ShapeDtypeStruct((64, 2048), BF16),...  94.5 us

profile of v5, /device:TPU:1, one launch (start us, length us, event | category | flops | bytes accessed | tf_op | source)
XLA Modules:
  0.0 96.2 jit_solution(1569616113964016766)
XLA Ops:
  0.0 94.5 %layer.1 = bf16[64,2048]{1,0:T(8,128)(2,1)} custom-call(bf16[256,256]{1,0:T(8,128)(2,1)} %q_ref.1, bf16[256,128]{1,0:T(8,128)(2,1)} %k_ref.1, bf16[256,128]{1,0:T(8,128)(2,1)} %v_ref.1, f32[256,128]{1,0:T(8,128)} %constant.8.clone.cosr_ref, f32[64,128]{1,0:T(8,128)} %constant.9.clone.cosc_ref, f32[256,128]{1,0:T(8,128)} %constant.10.clone.sinr_ref, ...), custom_call_target="tpu_custom_call" | custom-call | tf_op jit(solution)/shard_map/layer/pallas_call | solution.py:653
  94.5 1.7 %copy.19 = bf16[64,2048]{1,0:T(8,128)(2,1)} copy(bf16[64,2048]{1,0:T(8,128)(2,1)} %layer.1) | data formatting | bytes 524288
